TPU v7x, 256 devices: a whole 4x4x8 slice. The times are simulated.
256 devices in a mesh: sp: 32 (over z, x), tp: 8 (over y, core).
Axes of the slice: x: 4, y: 4, z: 8, core: 2. Of those that a mesh axis runs over, the one named last changes fastest.
Arguments:
- activations: bfloat16 [16384, 1024], P(('sp', 'tp')), may hold values from -8 to 8, as said below
- input_gain: float32 [1024], replicated, may hold values from 0.5 to 1.5
- query_weight: bfloat16 [1024, 1024], P(None, 'tp'), may hold values from -0.1875 to 0.1875
- key_weight: bfloat16 [1024, 1024], P(None, 'tp'), may hold values from -0.375 to 0.375
- value_weight: bfloat16 [1024, 1024], P(None, 'tp'), may hold values from -0.1875 to 0.1875
- stop_offset: float32 [16], P('tp'), may hold values from -16 to 0, as said below
- output_weight: bfloat16 [1024, 1024], P('tp'), may hold values from -0.1875 to 0.1875
- output_gain: float32 [1024], replicated, may hold values from 0.5 to 1.5
Outputs:
- layer_out: bfloat16 [16384, 1024], P(('sp', 'tp'))
Inputs may be any that keep to these rules, and one draw needn't show every extreme that they name: activations are noise of about unit size plus a mean vector of about unit size shared by each aligned block of 512 rows and different between runs; each row as a whole may also be scaled by a factor between 0.25 and 2; the result is clipped to the range. `stop_offset`: each entry equals minus the natural logarithm of 16384, minus 2, plus the natural logarithm of 3, plus a number between 0 and 0.7.
All inputs are finite; a program needn't handle non-finite values.
Results may differ from a plain program's by a relative error of at most 0.015.
Values may be sent and summed in bfloat16 or wider, within the bound.
A program may use at most 128 MiB of HBM per device.

v0:
```python
import jax
import jax.numpy as jnp
from jax import lax
from jax.sharding import PartitionSpec as P

epsilon = 1e-06


def over_all(shard, axis, dim, block):
    whole = lax.all_gather(shard, axis, axis=dim, tiled=True)
    return block(whole, jnp.int32(0))


def taken_in(shard, axis, dim, absorb, state):
    everything = jax.tree.map(lambda a: lax.all_gather(a, axis, axis=dim, tiled=True), shard)
    return absorb(state, everything, jnp.int32(0))


def own_rows_2(contribution, rows, axis):
    whole = contribution(jnp.int32(0), rows * lax.axis_size(axis)).astype(jnp.bfloat16)
    return lax.psum_scatter(whole, axis, scatter_dimension=0, tiled=True).astype(jnp.float32)


def scaled_rows(row_block, row_gain):
    widened = row_block.astype(jnp.float32)
    spread = jnp.mean(widened * widened, axis=-1, keepdims=True)
    return (widened * lax.rsqrt(spread + epsilon) * row_gain).astype(jnp.bfloat16)


def stopping_terms(queries, key_here, offsets, first_query, first_key):
    score_scale = queries.shape[-1] ** (-0.5)
    scores = jnp.einsum("thd,shd->hts", queries, key_here, preferred_element_type=jnp.float32)
    scores = scores * score_scale + offsets[:, None, None]
    query_pos = first_query + lax.iota(jnp.int32, queries.shape[0])
    key_pos = first_key + lax.iota(jnp.int32, key_here.shape[0])
    earlier = key_pos[None, :] < query_pos[:, None]
    log_keep = jnp.where(earlier[None], jax.nn.log_sigmoid(-scores), 0.0)
    return (scores, earlier, log_keep)


def shard_output(scores, earlier, log_keep, value_here):
    key_count = log_keep.shape[-1]
    upper_ones = (
        lax.iota(jnp.int32, key_count)[:, None] > lax.iota(jnp.int32, key_count)[None, :]
    ).astype(jnp.float32)
    within = jnp.dot(
        log_keep.reshape(-1, key_count), upper_ones, precision=lax.Precision.DEFAULT
    ).reshape(log_keep.shape)
    weights = jnp.where(earlier[None], jnp.exp(jax.nn.log_sigmoid(scores) + within), 0.0).astype(
        jnp.bfloat16
    )
    return jnp.einsum("hts,shd->thd", weights, value_here, preferred_element_type=jnp.float32)


def stick_factors(totals):
    prefix_sums = jnp.cumsum(totals, axis=0)
    return jnp.exp(prefix_sums[-1:] - prefix_sums)


def local(
    activations,
    input_gain,
    query_weight,
    key_weight,
    value_weight,
    stop_offset,
    output_weight,
    output_gain,
):
    normed = scaled_rows(activations, input_gain)
    heads_here = stop_offset.shape[0]
    head_dim = query_weight.shape[1] // heads_here

    def project(portion, offset):
        query_part = jnp.dot(portion, query_weight, preferred_element_type=jnp.float32).astype(
            jnp.bfloat16
        )
        key_part = jnp.dot(portion, key_weight, preferred_element_type=jnp.float32).astype(
            jnp.bfloat16
        )
        value_part = jnp.dot(portion, value_weight, preferred_element_type=jnp.float32).astype(
            jnp.bfloat16
        )
        return jnp.stack([query_part, key_part, value_part], axis=0)

    projected = over_all(normed, "tp", 0, project)
    block_len = projected.shape[1]
    queries = projected[0].reshape(block_len, heads_here, head_dim)
    key_rows = projected[1]
    value_rows = projected[2]
    blocks = lax.axis_size("sp")
    own_block = lax.axis_index("sp")
    first_query = own_block * block_len
    empty_totals = jnp.zeros((blocks, heads_here, block_len), jnp.float32)

    def split_shards(portion):
        return portion.reshape(portion.shape[0] // block_len, block_len, heads_here, head_dim)

    def add_totals(carried, portion, offset):
        key_shards = split_shards(portion)

        def add_shard(shard_index, current):
            block_index = offset // block_len + shard_index

            def compute_shard(present):
                scores, earlier, log_keep = stopping_terms(
                    queries,
                    key_shards[shard_index],
                    stop_offset,
                    first_query,
                    block_index * block_len,
                )
                return lax.dynamic_update_index_in_dim(
                    present, jnp.sum(log_keep, axis=-1), block_index, 0
                )

            def skip_shard(present):
                return present

            return lax.cond(block_index <= own_block, compute_shard, skip_shard, current)

        return lax.fori_loop(0, key_shards.shape[0], add_shard, carried)

    totals = taken_in(key_rows, "sp", 0, add_totals, empty_totals)
    factors = stick_factors(totals)

    def add_values(carried, portions, offset):
        key_shards = split_shards(portions[0])
        value_shards = split_shards(portions[1])

        def add_shard(shard_index, current):
            block_index = offset // block_len + shard_index

            def compute_shard(running):
                scores, earlier, log_keep = stopping_terms(
                    queries,
                    key_shards[shard_index],
                    stop_offset,
                    first_query,
                    block_index * block_len,
                )
                shard_part = shard_output(scores, earlier, log_keep, value_shards[shard_index])
                factor = lax.dynamic_index_in_dim(factors, block_index, 0, keepdims=False)
                return running + jnp.transpose(factor)[:, :, None] * shard_part

            def skip_shard(running):
                return running

            return lax.cond(block_index <= own_block, compute_shard, skip_shard, current)

        return lax.fori_loop(0, key_shards.shape[0], add_shard, carried)

    empty_running = jnp.zeros((block_len, heads_here, head_dim), jnp.float32)
    attended = taken_in((key_rows, value_rows), "sp", 0, add_values, empty_running)
    attended = attended.astype(jnp.bfloat16).reshape(block_len, heads_here * head_dim)
    own_rows = activations.shape[0]

    def project_out(offset, row_count):
        selected = lax.dynamic_slice_in_dim(attended, offset, row_count, 0)
        return jnp.dot(selected, output_weight, preferred_element_type=jnp.float32)

    summed = own_rows_2(project_out, own_rows, "tp")
    return scaled_rows(summed, output_gain)


def solution(mesh):
    in_specs = (
        P(("sp", "tp"), None),
        P(),
        P(None, "tp"),
        P(None, "tp"),
        P(None, "tp"),
        P("tp"),
        P("tp", None),
        P(),
    )
    out_specs = P(("sp", "tp"), None)
    return jax.shard_map(local, mesh=mesh, in_specs=in_specs, out_specs=out_specs, check_vma=False)
```

profile of v0, /device:TPU:231, one launch (start us, length us, event | category | flops | bytes accessed | tf_op | source)
XLA Modules:
  0.0 521.6 jit_solution(3619265038865059474)
XLA Ops:
  9.4 26.6 %all-gather.4.cloned.1.call-done = bf16[512,1024]{1,0:T(8,128)(2,1)} async-done(((bf16[64,1024]{1,0:T(8,128)(2,1)}), bf16[512,1024]{1,0:T(8,128)(2,1)}) %all-gather.4.cloned.1.call-update) | async-done | bytes 1048592 | tf_op jit(solution)/shard_map/all_gather | solution.py:10
  41.4 71.5 %all-gather.6.cloned.1.call-done = bf16[16384,128]{1,0:T(8,128)(2,1)} async-done(((bf16[512,128]{1,0:T(8,128)(2,1)}), bf16[16384,128]{1,0:T(8,128)(2,1)}) %all-gather.6.cloned.1.call-update) | async-done | bytes 4194320 | tf_op jit(solution)/shard_map/all_gather | solution.py:15
  112.9 14.7 %reshape.110 = bf16[32,512,2,64]{3,2,1,0:T(2,128)(2,1)} reshape(bf16[16384,128]{1,0:T(8,128)(2,1)} %all-gather.6.cloned.1.call-done) | data formatting | bytes 8388608 | tf_op jit(solution)/shard_map/reshape | solution.py:97
  127.6 18.3 %copy.15 = bf16[32,512,2,64]{1,3,2,0:T(8,128)(2,1)} copy(bf16[32,512,2,64]{3,2,1,0:T(2,128)(2,1)} %reshape.110) | data formatting | bytes 8388608 | tf_op jit(solution)/shard_map/while | solution.py:122
  146.0 98.3 %while.36 = (s32[]{:T(128)}, f32[32,2,512]{2,1,0:T(2,128)S(1)}, s32[]{:T(128)}, s32[]{:T(128)}, bf16[32,512,2,64]{1,3,2,0:T(8,128)(2,1)}, /*index=5*/bf16[512,2,64]{0,2,1:T(8,128)(2,1)S(1)}, f32[2]{0:T(128)S(1)}, s32[]{:T(128)}) while((s32[]{:T(128)}, f32[32,2,512]{2,1,0:T(2,128)S(1)}, s32[]{:T(128)}, s32[]{:T(128)}, ...), condition=%wide.region_5.6_spmd, body=%wide.region_1.5_spmd.sunk | while | flops 73138176 | bytes 807137 | solution.py:122
  244.4 14.8 %reshape.109 = bf16[32,512,2,64]{3,2,1,0:T(2,128)(2,1)} reshape(bf16[16384,128]{1,0:T(8,128)(2,1)} %all-gather.8.cloned.1.call-done) | data formatting | bytes 8388608 | tf_op jit(solution)/shard_map/reshape | solution.py:97
  259.2 18.4 %copy.17 = bf16[32,512,2,64]{1,3,2,0:T(8,128)(2,1)} copy(bf16[32,512,2,64]{3,2,1,0:T(2,128)(2,1)} %reshape.109) | data formatting | bytes 8388608 | tf_op jit(solution)/shard_map/while | solution.py:151
  277.6 198.6 %while.37 = (s32[]{:T(128)}, f32[512,2,64]{0,2,1:T(8,128)S(1)}, s32[]{:T(128)}, f32[32,2,512]{2,1,0:T(2,128)S(1)}, bf16[32,512,2,64]{1,3,2,0:T(8,128)(2,1)}, /*i...) while((s32[]{:T(128)}, f32[512,2,64]{0,2,1:T(8,128)S(1)}, ...), condition=%wide.region_10.11_spmd, body=%wide.region_7.10_spmd.sunk | while | flops 683803648 | bytes 8017149 | solution.py:151
  277.6 6.2 %conditional.5 = (f32[512,2,64]{0,2,1:T(8,128)S(1)}) conditional(s32[]{:T(128)} %convert_element_type.94, f32[512,2,64]{0,2,1:T(8,128)S(1)} %get-tuple-element.670, (s32[]{:T(128)}, f32[32,2,512]{2,1,0:T(2,128)S(1)}, bf16[32,512,2,64]{1,3,2,0:T(8,128)(2,1)}, s32[]{:T(128)}, bf16[32,512,2,64]{1,3,2,0:T(8,128)(2,1)}, ...), branch_computations={%region_8.8_spmd, %region_9.9_spmd} | conditional | flops 683803648 | bytes 8016970 | solution.py:149
  279.3 4.5 fusion.37
  283.8 6.2 %conditional.5 = (f32[512,2,64]{0,2,1:T(8,128)S(1)}) conditional(s32[]{:T(128)} %convert_element_type.94, f32[512,2,64]{0,2,1:T(8,128)S(1)} %get-tuple-element.670, (s32[]{:T(128)}, f32[32,2,512]{2,1,0:T(2,128)S(1)}, bf16[32,512,2,64]{1,3,2,0:T(8,128)(2,1)}, s32[]{:T(128)}, bf16[32,512,2,64]{1,3,2,0:T(8,128)(2,1)}, ...), branch_computations={%region_8.8_spmd, %region_9.9_spmd} | conditional | flops 683803648 | bytes 8016970 | solution.py:149
  290.0 6.2 %conditional.5 = (f32[512,2,64]{0,2,1:T(8,128)S(1)}) conditional(s32[]{:T(128)} %convert_element_type.94, f32[512,2,64]{0,2,1:T(8,128)S(1)} %get-tuple-element.670, (s32[]{:T(128)}, f32[32,2,512]{2,1,0:T(2,128)S(1)}, bf16[32,512,2,64]{1,3,2,0:T(8,128)(2,1)}, s32[]{:T(128)}, bf16[32,512,2,64]{1,3,2,0:T(8,128)(2,1)}, ...), branch_computations={%region_8.8_spmd, %region_9.9_spmd} | conditional | flops 683803648 | bytes 8016970 | solution.py:149
  291.7 4.5 fusion.37
  296.2 6.2 %conditional.5 = (f32[512,2,64]{0,2,1:T(8,128)S(1)}) conditional(s32[]{:T(128)} %convert_element_type.94, f32[512,2,64]{0,2,1:T(8,128)S(1)} %get-tuple-element.670, (s32[]{:T(128)}, f32[32,2,512]{2,1,0:T(2,128)S(1)}, bf16[32,512,2,64]{1,3,2,0:T(8,128)(2,1)}, s32[]{:T(128)}, bf16[32,512,2,64]{1,3,2,0:T(8,128)(2,1)}, ...), branch_computations={%region_8.8_spmd, %region_9.9_spmd} | conditional | flops 683803648 | bytes 8016970 | solution.py:149
  297.9 4.5 fusion.37
  302.4 6.2 %conditional.5 = (f32[512,2,64]{0,2,1:T(8,128)S(1)}) conditional(s32[]{:T(128)} %convert_element_type.94, f32[512,2,64]{0,2,1:T(8,128)S(1)} %get-tuple-element.670, (s32[]{:T(128)}, f32[32,2,512]{2,1,0:T(2,128)S(1)}, bf16[32,512,2,64]{1,3,2,0:T(8,128)(2,1)}, s32[]{:T(128)}, bf16[32,512,2,64]{1,3,2,0:T(8,128)(2,1)}, ...), branch_computations={%region_8.8_spmd, %region_9.9_spmd} | conditional | flops 683803648 | bytes 8016970 | solution.py:149
  304.1 4.5 fusion.37
  308.7 6.2 %conditional.5 = (f32[512,2,64]{0,2,1:T(8,128)S(1)}) conditional(s32[]{:T(128)} %convert_element_type.94, f32[512,2,64]{0,2,1:T(8,128)S(1)} %get-tuple-element.670, (s32[]{:T(128)}, f32[32,2,512]{2,1,0:T(2,128)S(1)}, bf16[32,512,2,64]{1,3,2,0:T(8,128)(2,1)}, s32[]{:T(128)}, bf16[32,512,2,64]{1,3,2,0:T(8,128)(2,1)}, ...), branch_computations={%region_8.8_spmd, %region_9.9_spmd} | conditional | flops 683803648 | bytes 8016970 | solution.py:149
  314.9 6.2 %conditional.5 = (f32[512,2,64]{0,2,1:T(8,128)S(1)}) conditional(s32[]{:T(128)} %convert_element_type.94, f32[512,2,64]{0,2,1:T(8,128)S(1)} %get-tuple-element.670, (s32[]{:T(128)}, f32[32,2,512]{2,1,0:T(2,128)S(1)}, bf16[32,512,2,64]{1,3,2,0:T(8,128)(2,1)}, s32[]{:T(128)}, bf16[32,512,2,64]{1,3,2,0:T(8,128)(2,1)}, ...), branch_computations={%region_8.8_spmd, %region_9.9_spmd} | conditional | flops 683803648 | bytes 8016970 | solution.py:149
  321.1 6.2 %conditional.5 = (f32[512,2,64]{0,2,1:T(8,128)S(1)}) conditional(s32[]{:T(128)} %convert_element_type.94, f32[512,2,64]{0,2,1:T(8,128)S(1)} %get-tuple-element.670, (s32[]{:T(128)}, f32[32,2,512]{2,1,0:T(2,128)S(1)}, bf16[32,512,2,64]{1,3,2,0:T(8,128)(2,1)}, s32[]{:T(128)}, bf16[32,512,2,64]{1,3,2,0:T(8,128)(2,1)}, ...), branch_computations={%region_8.8_spmd, %region_9.9_spmd} | conditional | flops 683803648 | bytes 8016970 | solution.py:149
  322.7 4.5 fusion.37
  327.3 6.2 %conditional.5 = (f32[512,2,64]{0,2,1:T(8,128)S(1)}) conditional(s32[]{:T(128)} %convert_element_type.94, f32[512,2,64]{0,2,1:T(8,128)S(1)} %get-tuple-element.670, (s32[]{:T(128)}, f32[32,2,512]{2,1,0:T(2,128)S(1)}, bf16[32,512,2,64]{1,3,2,0:T(8,128)(2,1)}, s32[]{:T(128)}, bf16[32,512,2,64]{1,3,2,0:T(8,128)(2,1)}, ...), branch_computations={%region_8.8_spmd, %region_9.9_spmd} | conditional | flops 683803648 | bytes 8016970 | solution.py:149
  328.9 4.5 fusion.37
  333.5 6.2 %conditional.5 = (f32[512,2,64]{0,2,1:T(8,128)S(1)}) conditional(s32[]{:T(128)} %convert_element_type.94, f32[512,2,64]{0,2,1:T(8,128)S(1)} %get-tuple-element.670, (s32[]{:T(128)}, f32[32,2,512]{2,1,0:T(2,128)S(1)}, bf16[32,512,2,64]{1,3,2,0:T(8,128)(2,1)}, s32[]{:T(128)}, bf16[32,512,2,64]{1,3,2,0:T(8,128)(2,1)}, ...), branch_computations={%region_8.8_spmd, %region_9.9_spmd} | conditional | flops 683803648 | bytes 8016970 | solution.py:149
  339.7 6.2 %conditional.5 = (f32[512,2,64]{0,2,1:T(8,128)S(1)}) conditional(s32[]{:T(128)} %convert_element_type.94, f32[512,2,64]{0,2,1:T(8,128)S(1)} %get-tuple-element.670, (s32[]{:T(128)}, f32[32,2,512]{2,1,0:T(2,128)S(1)}, bf16[32,512,2,64]{1,3,2,0:T(8,128)(2,1)}, s32[]{:T(128)}, bf16[32,512,2,64]{1,3,2,0:T(8,128)(2,1)}, ...), branch_computations={%region_8.8_spmd, %region_9.9_spmd} | conditional | flops 683803648 | bytes 8016970 | solution.py:149
  345.9 6.2 %conditional.5 = (f32[512,2,64]{0,2,1:T(8,128)S(1)}) conditional(s32[]{:T(128)} %convert_element_type.94, f32[512,2,64]{0,2,1:T(8,128)S(1)} %get-tuple-element.670, (s32[]{:T(128)}, f32[32,2,512]{2,1,0:T(2,128)S(1)}, bf16[32,512,2,64]{1,3,2,0:T(8,128)(2,1)}, s32[]{:T(128)}, bf16[32,512,2,64]{1,3,2,0:T(8,128)(2,1)}, ...), branch_computations={%region_8.8_spmd, %region_9.9_spmd} | conditional | flops 683803648 | bytes 8016970 | solution.py:149
  347.6 4.5 fusion.37
  352.1 6.2 %conditional.5 = (f32[512,2,64]{0,2,1:T(8,128)S(1)}) conditional(s32[]{:T(128)} %convert_element_type.94, f32[512,2,64]{0,2,1:T(8,128)S(1)} %get-tuple-element.670, (s32[]{:T(128)}, f32[32,2,512]{2,1,0:T(2,128)S(1)}, bf16[32,512,2,64]{1,3,2,0:T(8,128)(2,1)}, s32[]{:T(128)}, bf16[32,512,2,64]{1,3,2,0:T(8,128)(2,1)}, ...), branch_computations={%region_8.8_spmd, %region_9.9_spmd} | conditional | flops 683803648 | bytes 8016970 | solution.py:149
  358.3 6.2 %conditional.5 = (f32[512,2,64]{0,2,1:T(8,128)S(1)}) conditional(s32[]{:T(128)} %convert_element_type.94, f32[512,2,64]{0,2,1:T(8,128)S(1)} %get-tuple-element.670, (s32[]{:T(128)}, f32[32,2,512]{2,1,0:T(2,128)S(1)}, bf16[32,512,2,64]{1,3,2,0:T(8,128)(2,1)}, s32[]{:T(128)}, bf16[32,512,2,64]{1,3,2,0:T(8,128)(2,1)}, ...), branch_computations={%region_8.8_spmd, %region_9.9_spmd} | conditional | flops 683803648 | bytes 8016970 | solution.py:149
  364.5 6.2 %conditional.5 = (f32[512,2,64]{0,2,1:T(8,128)S(1)}) conditional(s32[]{:T(128)} %convert_element_type.94, f32[512,2,64]{0,2,1:T(8,128)S(1)} %get-tuple-element.670, (s32[]{:T(128)}, f32[32,2,512]{2,1,0:T(2,128)S(1)}, bf16[32,512,2,64]{1,3,2,0:T(8,128)(2,1)}, s32[]{:T(128)}, bf16[32,512,2,64]{1,3,2,0:T(8,128)(2,1)}, ...), branch_computations={%region_8.8_spmd, %region_9.9_spmd} | conditional | flops 683803648 | bytes 8016970 | solution.py:149
  370.7 6.2 %conditional.5 = (f32[512,2,64]{0,2,1:T(8,128)S(1)}) conditional(s32[]{:T(128)} %convert_element_type.94, f32[512,2,64]{0,2,1:T(8,128)S(1)} %get-tuple-element.670, (s32[]{:T(128)}, f32[32,2,512]{2,1,0:T(2,128)S(1)}, bf16[32,512,2,64]{1,3,2,0:T(8,128)(2,1)}, s32[]{:T(128)}, bf16[32,512,2,64]{1,3,2,0:T(8,128)(2,1)}, ...), branch_computations={%region_8.8_spmd, %region_9.9_spmd} | conditional | flops 683803648 | bytes 8016970 | solution.py:149
  376.9 6.2 %conditional.5 = (f32[512,2,64]{0,2,1:T(8,128)S(1)}) conditional(s32[]{:T(128)} %convert_element_type.94, f32[512,2,64]{0,2,1:T(8,128)S(1)} %get-tuple-element.670, (s32[]{:T(128)}, f32[32,2,512]{2,1,0:T(2,128)S(1)}, bf16[32,512,2,64]{1,3,2,0:T(8,128)(2,1)}, s32[]{:T(128)}, bf16[32,512,2,64]{1,3,2,0:T(8,128)(2,1)}, ...), branch_computations={%region_8.8_spmd, %region_9.9_spmd} | conditional | flops 683803648 | bytes 8016970 | solution.py:149
  383.1 6.2 %conditional.5 = (f32[512,2,64]{0,2,1:T(8,128)S(1)}) conditional(s32[]{:T(128)} %convert_element_type.94, f32[512,2,64]{0,2,1:T(8,128)S(1)} %get-tuple-element.670, (s32[]{:T(128)}, f32[32,2,512]{2,1,0:T(2,128)S(1)}, bf16[32,512,2,64]{1,3,2,0:T(8,128)(2,1)}, s32[]{:T(128)}, bf16[32,512,2,64]{1,3,2,0:T(8,128)(2,1)}, ...), branch_computations={%region_8.8_spmd, %region_9.9_spmd} | conditional | flops 683803648 | bytes 8016970 | solution.py:149
  389.3 6.2 %conditional.5 = (f32[512,2,64]{0,2,1:T(8,128)S(1)}) conditional(s32[]{:T(128)} %convert_element_type.94, f32[512,2,64]{0,2,1:T(8,128)S(1)} %get-tuple-element.670, (s32[]{:T(128)}, f32[32,2,512]{2,1,0:T(2,128)S(1)}, bf16[32,512,2,64]{1,3,2,0:T(8,128)(2,1)}, s32[]{:T(128)}, bf16[32,512,2,64]{1,3,2,0:T(8,128)(2,1)}, ...), branch_computations={%region_8.8_spmd, %region_9.9_spmd} | conditional | flops 683803648 | bytes 8016970 | solution.py:149
  395.5 6.2 %conditional.5 = (f32[512,2,64]{0,2,1:T(8,128)S(1)}) conditional(s32[]{:T(128)} %convert_element_type.94, f32[512,2,64]{0,2,1:T(8,128)S(1)} %get-tuple-element.670, (s32[]{:T(128)}, f32[32,2,512]{2,1,0:T(2,128)S(1)}, bf16[32,512,2,64]{1,3,2,0:T(8,128)(2,1)}, s32[]{:T(128)}, bf16[32,512,2,64]{1,3,2,0:T(8,128)(2,1)}, ...), branch_computations={%region_8.8_spmd, %region_9.9_spmd} | conditional | flops 683803648 | bytes 8016970 | solution.py:149
  401.7 6.2 %conditional.5 = (f32[512,2,64]{0,2,1:T(8,128)S(1)}) conditional(s32[]{:T(128)} %convert_element_type.94, f32[512,2,64]{0,2,1:T(8,128)S(1)} %get-tuple-element.670, (s32[]{:T(128)}, f32[32,2,512]{2,1,0:T(2,128)S(1)}, bf16[32,512,2,64]{1,3,2,0:T(8,128)(2,1)}, s32[]{:T(128)}, bf16[32,512,2,64]{1,3,2,0:T(8,128)(2,1)}, ...), branch_computations={%region_8.8_spmd, %region_9.9_spmd} | conditional | flops 683803648 | bytes 8016970 | solution.py:149
  408.0 6.2 %conditional.5 = (f32[512,2,64]{0,2,1:T(8,128)S(1)}) conditional(s32[]{:T(128)} %convert_element_type.94, f32[512,2,64]{0,2,1:T(8,128)S(1)} %get-tuple-element.670, (s32[]{:T(128)}, f32[32,2,512]{2,1,0:T(2,128)S(1)}, bf16[32,512,2,64]{1,3,2,0:T(8,128)(2,1)}, s32[]{:T(128)}, bf16[32,512,2,64]{1,3,2,0:T(8,128)(2,1)}, ...), branch_computations={%region_8.8_spmd, %region_9.9_spmd} | conditional | flops 683803648 | bytes 8016970 | solution.py:149
  414.2 6.2 %conditional.5 = (f32[512,2,64]{0,2,1:T(8,128)S(1)}) conditional(s32[]{:T(128)} %convert_element_type.94, f32[512,2,64]{0,2,1:T(8,128)S(1)} %get-tuple-element.670, (s32[]{:T(128)}, f32[32,2,512]{2,1,0:T(2,128)S(1)}, bf16[32,512,2,64]{1,3,2,0:T(8,128)(2,1)}, s32[]{:T(128)}, bf16[32,512,2,64]{1,3,2,0:T(8,128)(2,1)}, ...), branch_computations={%region_8.8_spmd, %region_9.9_spmd} | conditional | flops 683803648 | bytes 8016970 | solution.py:149
  420.4 6.2 %conditional.5 = (f32[512,2,64]{0,2,1:T(8,128)S(1)}) conditional(s32[]{:T(128)} %convert_element_type.94, f32[512,2,64]{0,2,1:T(8,128)S(1)} %get-tuple-element.670, (s32[]{:T(128)}, f32[32,2,512]{2,1,0:T(2,128)S(1)}, bf16[32,512,2,64]{1,3,2,0:T(8,128)(2,1)}, s32[]{:T(128)}, bf16[32,512,2,64]{1,3,2,0:T(8,128)(2,1)}, ...), branch_computations={%region_8.8_spmd, %region_9.9_spmd} | conditional | flops 683803648 | bytes 8016970 | solution.py:149
  426.6 6.2 %conditional.5 = (f32[512,2,64]{0,2,1:T(8,128)S(1)}) conditional(s32[]{:T(128)} %convert_element_type.94, f32[512,2,64]{0,2,1:T(8,128)S(1)} %get-tuple-element.670, (s32[]{:T(128)}, f32[32,2,512]{2,1,0:T(2,128)S(1)}, bf16[32,512,2,64]{1,3,2,0:T(8,128)(2,1)}, s32[]{:T(128)}, bf16[32,512,2,64]{1,3,2,0:T(8,128)(2,1)}, ...), branch_computations={%region_8.8_spmd, %region_9.9_spmd} | conditional | flops 683803648 | bytes 8016970 | solution.py:149
  432.8 6.2 %conditional.5 = (f32[512,2,64]{0,2,1:T(8,128)S(1)}) conditional(s32[]{:T(128)} %convert_element_type.94, f32[512,2,64]{0,2,1:T(8,128)S(1)} %get-tuple-element.670, (s32[]{:T(128)}, f32[32,2,512]{2,1,0:T(2,128)S(1)}, bf16[32,512,2,64]{1,3,2,0:T(8,128)(2,1)}, s32[]{:T(128)}, bf16[32,512,2,64]{1,3,2,0:T(8,128)(2,1)}, ...), branch_computations={%region_8.8_spmd, %region_9.9_spmd} | conditional | flops 683803648 | bytes 8016970 | solution.py:149
  439.0 6.2 %conditional.5 = (f32[512,2,64]{0,2,1:T(8,128)S(1)}) conditional(s32[]{:T(128)} %convert_element_type.94, f32[512,2,64]{0,2,1:T(8,128)S(1)} %get-tuple-element.670, (s32[]{:T(128)}, f32[32,2,512]{2,1,0:T(2,128)S(1)}, bf16[32,512,2,64]{1,3,2,0:T(8,128)(2,1)}, s32[]{:T(128)}, bf16[32,512,2,64]{1,3,2,0:T(8,128)(2,1)}, ...), branch_computations={%region_8.8_spmd, %region_9.9_spmd} | conditional | flops 683803648 | bytes 8016970 | solution.py:149
  445.2 6.2 %conditional.5 = (f32[512,2,64]{0,2,1:T(8,128)S(1)}) conditional(s32[]{:T(128)} %convert_element_type.94, f32[512,2,64]{0,2,1:T(8,128)S(1)} %get-tuple-element.670, (s32[]{:T(128)}, f32[32,2,512]{2,1,0:T(2,128)S(1)}, bf16[32,512,2,64]{1,3,2,0:T(8,128)(2,1)}, s32[]{:T(128)}, bf16[32,512,2,64]{1,3,2,0:T(8,128)(2,1)}, ...), branch_computations={%region_8.8_spmd, %region_9.9_spmd} | conditional | flops 683803648 | bytes 8016970 | solution.py:149
  451.4 6.2 %conditional.5 = (f32[512,2,64]{0,2,1:T(8,128)S(1)}) conditional(s32[]{:T(128)} %convert_element_type.94, f32[512,2,64]{0,2,1:T(8,128)S(1)} %get-tuple-element.670, (s32[]{:T(128)}, f32[32,2,512]{2,1,0:T(2,128)S(1)}, bf16[32,512,2,64]{1,3,2,0:T(8,128)(2,1)}, s32[]{:T(128)}, bf16[32,512,2,64]{1,3,2,0:T(8,128)(2,1)}, ...), branch_computations={%region_8.8_spmd, %region_9.9_spmd} | conditional | flops 683803648 | bytes 8016970 | solution.py:149
  457.6 6.2 %conditional.5 = (f32[512,2,64]{0,2,1:T(8,128)S(1)}) conditional(s32[]{:T(128)} %convert_element_type.94, f32[512,2,64]{0,2,1:T(8,128)S(1)} %get-tuple-element.670, (s32[]{:T(128)}, f32[32,2,512]{2,1,0:T(2,128)S(1)}, bf16[32,512,2,64]{1,3,2,0:T(8,128)(2,1)}, s32[]{:T(128)}, bf16[32,512,2,64]{1,3,2,0:T(8,128)(2,1)}, ...), branch_computations={%region_8.8_spmd, %region_9.9_spmd} | conditional | flops 683803648 | bytes 8016970 | solution.py:149
  463.8 6.2 %conditional.5 = (f32[512,2,64]{0,2,1:T(8,128)S(1)}) conditional(s32[]{:T(128)} %convert_element_type.94, f32[512,2,64]{0,2,1:T(8,128)S(1)} %get-tuple-element.670, (s32[]{:T(128)}, f32[32,2,512]{2,1,0:T(2,128)S(1)}, bf16[32,512,2,64]{1,3,2,0:T(8,128)(2,1)}, s32[]{:T(128)}, bf16[32,512,2,64]{1,3,2,0:T(8,128)(2,1)}, ...), branch_computations={%region_8.8_spmd, %region_9.9_spmd} | conditional | flops 683803648 | bytes 8016970 | solution.py:149
  470.0 6.2 %conditional.5 = (f32[512,2,64]{0,2,1:T(8,128)S(1)}) conditional(s32[]{:T(128)} %convert_element_type.94, f32[512,2,64]{0,2,1:T(8,128)S(1)} %get-tuple-element.670, (s32[]{:T(128)}, f32[32,2,512]{2,1,0:T(2,128)S(1)}, bf16[32,512,2,64]{1,3,2,0:T(8,128)(2,1)}, s32[]{:T(128)}, bf16[32,512,2,64]{1,3,2,0:T(8,128)(2,1)}, ...), branch_computations={%region_8.8_spmd, %region_9.9_spmd} | conditional | flops 683803648 | bytes 8016970 | solution.py:149
  477.7 34.7 %reduce-scatter.2.cloned.1.call-done = bf16[64,1024]{1,0:T(8,128)(2,1)} async-done(((bf16[512,1024]{1,0:T(8,128)(2,1)}), bf16[64,1024]{1,0:T(8,128)(2,1)}) %reduce-scatter.2.cloned.1.call-update) | async-done | bytes 131088 | tf_op jit(solution)/shard_map/reduce_scatter | solution.py:21
  (351 shorter events, 370.5 us)
Async XLA Ops:
  6.5 469.7 %copy-start = (bf16[128,1024]{1,0:T(8,128)(2,1)S(1)}, bf16[128,1024]{1,0:T(8,128)(2,1)}, u32[]{:S(2)}) copy-start(bf16[128,1024]{1,0:T(8,128)(2,1)} %param.22) | copy-start | bytes 786436
  6.5 32.0 %copy-start.2 = (bf16[1024,128]{1,0:T(8,128)(2,1)S(1)}, bf16[1024,128]{1,0:T(8,128)(2,1)}, u32[]{:S(2)}) copy-start(bf16[1024,128]{1,0:T(8,128)(2,1)} %param.20) | copy-start | bytes 786436
  6.5 34.4 %copy-start.3 = (bf16[1024,128]{1,0:T(8,128)(2,1)S(1)}, bf16[1024,128]{1,0:T(8,128)(2,1)}, u32[]{:S(2)}) copy-start(bf16[1024,128]{1,0:T(8,128)(2,1)} %param.18) | copy-start | bytes 786436
  6.5 29.4 %all-gather.4.cloned.1.call-start = ((), (), s32[]{:S(2)}) async-start(), calls=%async_computation.1 | async-start | bytes 1179648 | tf_op jit(solution)/shard_map/all_gather | solution.py:10
  9.4 103.5 %all-gather.6.cloned.1.call-start = ((), (), s32[]{:S(2)}) async-start(), calls=%async_computation.2 | async-start | bytes 4325376 | tf_op jit(solution)/shard_map/all_gather | solution.py:15
  36.0 4.9 copy-start.1
  38.5 206.0 %all-gather.8.cloned.1.call-start = ((), (), s32[]{:S(2)}) async-start(), calls=%async_computation.3 | async-start | bytes 4325376 | tf_op jit(solution)/shard_map/all_gather | solution.py:15
  40.8 471.6 %reduce-scatter.2.cloned.1.call-start = ((), (), s32[]{:S(2)}) async-start(), calls=%async_computation.4 | async-start | bytes 1179648 | tf_op jit(solution)/shard_map/reduce_scatter | solution.py:21
  127.6 18.4 %copy-start.5 = (f32[2]{0:T(128)S(1)}, f32[2]{0:T(128)}, u32[]{:S(2)}) copy-start(f32[2]{0:T(128)} %param.21) | copy-start | bytes 28
  476.2 37.2 %copy-start.4 = (f32[1024]{0:T(1024)S(1)}, f32[1024]{0:T(1024)}, u32[]{:S(2)}) copy-start(f32[1024]{0:T(1024)} %param.23) | copy-start | bytes 12292
Sparse Core Ops, SparseCore 0:
  9.5 26.4 all-gather.3
  38.6 74.2 all-gather.5
  115.5 78.6 all-gather.7
  477.8 34.5 reduce-scatter.1
where the time goes:
time: 530 us; the launch traced here: 522 us
  matrix products  284 us (54%)
  waiting for transfers between devices  133 us (25%)
  local copies, waits for them, and re-layouts  67 us (13%)
  other arithmetic  19.7 us (4%)
  between operations  13.3 us (3%)
    dot_general x32, matrix products, shard_output(): jnp.einsum('hts,shd->thd', weights, value_here, preferred_element_type=jn...  144 us
    dot_general x64, matrix products, stopping_terms(): jnp.einsum('thd,shd->hts', queries, key_here, preferred_element_type=jnp....  133 us
    all_gather x2, waiting for transfers between devices, taken_in(): lax.all_gather(a, axis, axis=dim, tiled=True)  71.5 us
    reduce_scatter x1, waiting for transfers between devices, own_rows_2(): lax.psum_scatter(whole, axis, scatter_dimension=0, tiled=True)  34.7 us
    reshape x2, local copies, waits for them, and re-layouts, split_shards(): portion.reshape(portion.shape[0] // block_len, block_len, heads_here, hea...  29.5 us
    all_gather x1, waiting for transfers between devices, over_all(): whole = lax.all_gather(shard, axis, axis=dim, tiled=True)  26.6 us
    while x1, local copies, waits for them, and re-layouts, add_values(): return lax.fori_loop(0, key_shards.shape[0], add_shard, carried)  18.4 us
    while x1, local copies, waits for them, and re-layouts, add_totals(): return lax.fori_loop(0, key_shards.shape[0], add_shard, carried)  18.3 us
  transfers between devices with their start and end apart: 4, of which 3 were waited for; matrix products, arithmetic and copies ran while one was open for 25% of the time, Pallas kernels for 0%

commit v1 on v0

v1 whole, which is shorter than its diff:
```python
import functools

import jax
import jax.numpy as jnp
from jax import lax
from jax.experimental import pallas as pl
from jax.experimental.pallas import tpu as pltpu
from jax.sharding import PartitionSpec as P

epsilon = 1e-06
LANES = 128
SUB = 8
NT = (((1,), (1,)), ((), ()))


def scaled_rows(row_block, row_gain):
    widened = row_block.astype(jnp.float32)
    spread = jnp.mean(widened * widened, axis=-1, keepdims=True)
    return (widened * lax.rsqrt(spread + epsilon) * row_gain).astype(jnp.bfloat16)


def head_operands(raw, offset, h, half):
    lane = lax.broadcasted_iota(jnp.int32, raw.shape, 1)
    mine = (lane >= h * half) & (lane < (h + 1) * half)
    base = (1 - h) * half
    first = jnp.full(raw.shape, offset, jnp.float32)
    one = first.astype(jnp.bfloat16)
    rest = first - one.astype(jnp.float32)
    two = rest.astype(jnp.bfloat16)
    three = (rest - two.astype(jnp.float32)).astype(jnp.bfloat16)
    parts = jnp.where(lane == base, one, jnp.where(lane == base + 1, two, jnp.where(lane == base + 2, three, jnp.zeros_like(one))))
    return jnp.where(mine, raw, parts)


def key_operand(k, h, half):
    lane = lax.broadcasted_iota(jnp.int32, k.shape, 1)
    mine = (lane >= h * half) & (lane < (h + 1) * half)
    base = (1 - h) * half
    ones = jnp.where((lane >= base) & (lane < base + 3), jnp.ones_like(k), jnp.zeros_like(k))
    return jnp.where(mine, k, ones)


def suffix_products(total):
    row = lax.broadcasted_iota(jnp.int32, total.shape, 0)
    one = jnp.ones_like(total)

    def up(x, k):
        return jnp.where(row < SUB - k, pltpu.roll(x, SUB - k, 0), one)

    y = up(total, 1)
    y = y * up(y, 1)
    y = y * up(y, 2)
    return y * up(y, 4)


def tile_weights(halved, carry):
    keys, n = halved.shape
    steps = keys // SUB
    t = jnp.tanh(halved)
    take = 1.0 + t
    keep = 1.0 - t
    run = jnp.ones((SUB, n), jnp.float32)
    local = [None] * steps
    for v in reversed(range(steps)):
        local[v] = take[v * SUB : (v + 1) * SUB] * run
        run = run * keep[v * SUB : (v + 1) * SUB]
    total = run * (2.0 ** -steps)
    factor = suffix_products(total) * carry
    after = factor * total
    carry = jnp.broadcast_to(after[0:1], (SUB, n))
    return jnp.concatenate([x * factor for x in local], axis=0).astype(jnp.bfloat16), carry


def attention_kernel(off_ref, q_ref, kp_ref, vt_ref, out_ref, qh_ref, acc_ref, carry_ref):
    half = q_ref.shape[1] // 2
    block = q_ref.shape[0]
    me = lax.axis_index("sp")
    for h in range(2):
        qh_ref[h] = head_operands(q_ref[...], off_ref[h] * 0.5, h, half)
    acc_ref[...] = jnp.zeros_like(acc_ref)
    carry_ref[...] = jnp.ones_like(carry_ref)

    def tile(kb, h, diagonal):
        kh = key_operand(kp_ref[kb], h, half)
        halved = lax.dot_general(kh, qh_ref[h], NT, preferred_element_type=jnp.float32)
        if diagonal:
            row = lax.broadcasted_iota(jnp.int32, halved.shape, 0)
            query = lax.broadcasted_iota(jnp.int32, halved.shape, 1)
            key = lax.rem(row, SUB) * (block // SUB) + lax.div(row, SUB)
            halved = jnp.where(key < query, halved, -1e9)
        weights, carry_ref[h] = tile_weights(halved, carry_ref[h])
        acc_ref[h * half : (h + 1) * half] += jnp.dot(
            vt_ref[kb, h * half : (h + 1) * half], weights, preferred_element_type=jnp.float32
        )

    for h in range(2):
        tile(me, h, True)

    def body(i, c):
        for h in range(2):
            tile(me - 1 - i, h, False)
        return c

    lax.fori_loop(0, me, body, 0)
    out_ref[...] = jnp.transpose(acc_ref[...]).astype(out_ref.dtype)


def local(activations, input_gain, query_weight, key_weight, value_weight, stop_offset, output_weight, output_gain):
    normed = scaled_rows(activations, input_gain)
    whole = lax.all_gather(normed, "tp", axis=0, tiled=True)

    def proj(w):
        return jnp.dot(whole, w, preferred_element_type=jnp.float32).astype(jnp.bfloat16)

    q = proj(query_weight) * jnp.bfloat16(0.0625)
    k, v = proj(key_weight), proj(value_weight)
    block, width = q.shape
    steps = block // SUB
    perm = lambda a: a.reshape(SUB, steps, width).transpose(1, 0, 2).reshape(block, width)
    scale = jnp.repeat(2.0 ** -(steps - jnp.arange(steps, dtype=jnp.float32)), SUB)
    kp = perm(k)
    vt = (perm(v) * scale[:, None].astype(jnp.bfloat16)).T
    kp = lax.all_gather(kp, "sp", axis=0, tiled=False)
    vt = lax.all_gather(vt, "sp", axis=0, tiled=False)
    attended = pl.pallas_call(
        attention_kernel,
        out_shape=jax.ShapeDtypeStruct((block, width), jnp.bfloat16),
        in_specs=[pl.BlockSpec(memory_space=pltpu.SMEM)] + [pl.BlockSpec(memory_space=pltpu.VMEM)] * 3,
        out_specs=pl.BlockSpec(memory_space=pltpu.VMEM),
        scratch_shapes=[
            pltpu.VMEM((2, block, width), jnp.bfloat16),
            pltpu.VMEM((width, block), jnp.float32),
            pltpu.VMEM((2, SUB, block), jnp.float32),
        ],
        compiler_params=pltpu.CompilerParams(vmem_limit_bytes=48 * 1024 * 1024),
    )(stop_offset, q, kp, vt)
    out = jnp.dot(attended, output_weight, preferred_element_type=jnp.float32).astype(jnp.bfloat16)
    summed = lax.psum_scatter(out, "tp", scatter_dimension=0, tiled=True).astype(jnp.float32)
    return scaled_rows(summed, output_gain)


def solution(mesh):
    in_specs = (P(("sp", "tp"), None), P(), P(None, "tp"), P(None, "tp"), P(None, "tp"), P("tp"), P("tp", None), P())
    return jax.shard_map(local, mesh=mesh, in_specs=in_specs, out_specs=P(("sp", "tp"), None), check_vma=False)
```

time: 530 us -> 292 us (0.55)
  matrix products: 284 us -> 6.45 us
  waiting for transfers between devices: 133 us -> 210 us
  local copies, waits for them, and re-layouts: 67 us -> 9.59 us
  Pallas kernels: 0 us -> 40.7 us
  other arithmetic: 19.7 us -> 6.27 us
    dot_general x100 -> x4, matrix products: 284 us -> 6.45 us  [the longest x3 5.06 us: proj(): jnp.dot(whole, w, preferred_element_type=jnp.float32).astype(jnp.bfloat16)]
    all_gather x3, waiting for transfers between devices: 98.1 us -> 176 us  [the longest x1 76.3 us: local(): kp = lax.all_gather(kp, 'sp', axis=0, tiled=False)]
    pallas_call x0 -> x1, Pallas kernels: none -> 40.7 us  [local(): pl.pallas_call(attention_kernel, out_shape=jax.ShapeDtypeStruct((block, w...]
    while x2 -> x0, local copies, waits for them, and re-layouts: 36.7 us -> none  [the longest x1 18.4 us: add_values(): return lax.fori_loop(0, key_shards.shape[0], add_shard, carried)]
    reshape x2 -> x0, local copies, waits for them, and re-layouts: 29.5 us -> none  [split_shards(): portion.reshape(portion.shape[0] // block_len, block_len, heads_here, hea...]
    lt x64 -> x0, other arithmetic: 13.7 us -> none  [stopping_terms(): earlier = key_pos[None, :] < query_pos[:, None]]
    all_gather x0 -> x1, local copies, waits for them, and re-layouts: none -> 6.46 us  [local(): vt = lax.all_gather(vt, 'sp', axis=0, tiled=False)]
  transfers between devices with their start and end apart: 4 -> 4, of which waited for: 3 -> 4; matrix products, arithmetic and copies ran while one was open for 25% -> 4% of each run, Pallas kernels for 0% -> 0%
where the time goes in v1:
time: 292 us; the launch traced here: 287 us
  waiting for transfers between devices  210 us (72%)
  Pallas kernels  40.7 us (14%)
  between operations  13.2 us (5%)
  local copies, waits for them, and re-layouts  9.59 us (3%)
  matrix products  6.45 us (2%)
  other arithmetic  6.27 us (2%)
    all_gather x1, waiting for transfers between devices, local(): kp = lax.all_gather(kp, 'sp', axis=0, tiled=False)  76.3 us
    all_gather x1, waiting for transfers between devices, local(): vt = lax.all_gather(vt, 'sp', axis=0, tiled=False)  73.1 us
    pallas_call x1, Pallas kernels, local(): pl.pallas_call(attention_kernel, out_shape=jax.ShapeDtypeStruct((block, w...  40.7 us
    reduce_scatter x1, waiting for transfers between devices, local(): lax.psum_scatter(out, 'tp', scatter_dimension=0, tiled=True)  34.6 us
    all_gather x1, waiting for transfers between devices, local(): whole = lax.all_gather(normed, 'tp', axis=0, tiled=True)  26.4 us
    all_gather x1, local copies, waits for them, and re-layouts, local(): vt = lax.all_gather(vt, 'sp', axis=0, tiled=False)  6.46 us
  transfers between devices with their start and end apart: 4, of which 4 were waited for; matrix products, arithmetic and copies ran while one was open for 4% of the time, Pallas kernels for 0%

profile of v1, /device:TPU:231, one launch (start us, length us, event | category | flops | bytes accessed | tf_op | source)
XLA Modules:
  0.0 286.8 jit_solution(18262484241140362252)
XLA Ops:
  6.5 0.0 copy-start
  6.5 0.0 copy-start.3
  6.5 0.0 all-gather.5.cloned.1.call-start
  6.5 1.1 fusion.1
  7.6 1.7 fusion.3
  9.3 0.0 all-gather.5.cloned.1.call-update
  9.3 0.0 all-gather.9.cloned.1.call-start
  9.4 0.1 broadcast_in_dim.2
  9.5 0.1 convert_element_type.42
  9.6 26.4 %all-gather.5.cloned.1.call-done = bf16[512,1024]{1,0:T(8,128)(2,1)} async-done(((bf16[64,1024]{1,0:T(8,128)(2,1)}), bf16[512,1024]{1,0:T(8,128)(2,1)}) %all-gather.5.cloned.1.call-update) | async-done | bytes 1048592 | tf_op jit(solution)/shard_map/all_gather | solution.py:110
  36.0 1.7 convolution_convert_fusion.1
  37.7 0.8 fusion.7
  38.5 0.0 all-gather.9.cloned.1.call-update
  38.5 0.0 all-gather.7.cloned.1.call-start
  38.5 1.7 convolution_convert_fusion.2
  40.2 0.7 copy.19
  41.0 0.0 all-gather.7.cloned.1.call-update
  41.0 0.0 reduce-scatter.2.cloned.1.call-start
  41.1 0.0 copy-done.3
  41.1 1.7 fusion.q_ref
  42.7 0.0 copy-start.2
  42.8 73.1 %all-gather.9.cloned.1.call-done = bf16[4096,512]{0,1:T(8,128)(2,1)} async-done(((bf16[128,512]{0,1:T(8,128)(2,1)}), bf16[4096,512]{0,1:T(8,128)(2,1)}) %all-gather.9.cloned.1.call-update) | async-done | bytes 4194320 | tf_op jit(solution)/shard_map/all_gather | solution.py:124
  115.8 6.5 %copy.16 = bf16[4096,512]{1,0:T(8,128)(2,1)} copy(bf16[4096,512]{0,1:T(8,128)(2,1)} %all-gather.9.cloned.1.call-done) | data formatting | bytes 8388608 | tf_op jit(solution)/shard_map/all_gather | solution.py:124
  122.3 76.3 %all-gather.7.cloned.1.call-done.kp_ref = bf16[32,512,128]{2,1,0:T(8,128)(2,1)} async-done(((bf16[1,512,128]{2,1,0:T(8,128)(2,1)}), bf16[32,512,128]{2,1,0:T(8,128)(2,1)}) %all-gather.7.cloned.1.call-update) | async-done | bytes 4194320 | tf_op jit(solution)/shard_map/all_gather | solution.py:123
  198.6 0.0 copy-done.2
  198.6 0.0 copy-start.1
  198.6 2.2 copy-done.1
  200.8 0.0 copy-start.4
  200.8 40.7 %shard_map.82 = bf16[512,128]{1,0:T(8,128)(2,1)S(1)} custom-call(f32[2]{0:T(128)S(1)} %copy-done.2, bf16[512,128]{1,0:T(8,128)(2,1)S(1)} %fusion.q_ref, bf16[32,512,128]{2,1,0:T(8,128)(2,1)S(1)} %copy-done.1, bf16[32,128,512]{2,1,0:T(8,128)(2,1)} %bitcast.24), custom_call_target="tpu_custom_call" | custom-call | tf_op jit(solution)/shard_map/pallas_call | solution.py:125
  241.5 0.0 copy-done
  241.5 1.4 convolution_convert_fusion
  242.9 0.0 reduce-scatter.2.cloned.1.call-update
  242.9 34.6 %reduce-scatter.2.cloned.1.call-done = bf16[64,1024]{1,0:T(8,128)(2,1)} async-done(((bf16[512,1024]{1,0:T(8,128)(2,1)}), bf16[64,1024]{1,0:T(8,128)(2,1)}) %reduce-scatter.2.cloned.1.call-update) | async-done | bytes 131088 | tf_op jit(solution)/shard_map/reduce_scatter | solution.py:138
  277.6 1.0 fusion.4
  278.6 0.0 copy-done.4
  278.6 1.7 fusion.6
  (3 shorter events, 0.0 us)
Async XLA Ops:
  6.5 235.0 %copy-start = (bf16[128,1024]{1,0:T(8,128)(2,1)S(1)}, bf16[128,1024]{1,0:T(8,128)(2,1)}, u32[]{:S(2)}) copy-start(bf16[128,1024]{1,0:T(8,128)(2,1)} %param.14) | copy-start | bytes 786436
  6.5 34.5 %copy-start.3 = (bf16[1024,128]{1,0:T(8,128)(2,1)S(1)}, bf16[1024,128]{1,0:T(8,128)(2,1)}, u32[]{:S(2)}) copy-start(bf16[1024,128]{1,0:T(8,128)(2,1)} %param.10) | copy-start | bytes 786436
  6.5 29.4 %all-gather.5.cloned.1.call-start = ((), (), s32[]{:S(2)}) async-start(), calls=%async_computation.1 | async-start | bytes 1179648 | tf_op jit(solution)/shard_map/all_gather | solution.py:110
  9.3 106.5 %all-gather.9.cloned.1.call-start = ((), (), s32[]{:S(2)}) async-start(), calls=%async_computation.4 | async-start | bytes 4325376 | tf_op jit(solution)/shard_map/all_gather | solution.py:124
  38.5 160.1 %all-gather.7.cloned.1.call-start = ((), (), s32[]{:S(2)}) async-start(), calls=%async_computation.2 | async-start | bytes 4325376 | tf_op jit(solution)/shard_map/all_gather | solution.py:123
  41.0 236.6 %reduce-scatter.2.cloned.1.call-start = ((), (), s32[]{:S(2)}) async-start(), calls=%async_computation.3 | async-start | bytes 1179648 | tf_op jit(solution)/shard_map/reduce_scatter | solution.py:138
  42.7 155.9 %copy-start.2 = (f32[2]{0:T(128)S(1)}, f32[2]{0:T(128)}, u32[]{:S(2)}) copy-start(f32[2]{0:T(128)} %off_ref.1) | copy-start | bytes 28
  198.6 2.2 copy-start.1
  200.8 77.8 %copy-start.4 = (f32[1024]{0:T(1024)S(1)}, f32[1024]{0:T(1024)}, u32[]{:S(2)}) copy-start(f32[1024]{0:T(1024)} %param.15) | copy-start | bytes 12292
Sparse Core Ops, SparseCore 0:
  9.5 26.4 all-gather.4
  38.6 77.1 all-gather.8
  118.4 80.1 all-gather.6
  243.1 34.4 reduce-scatter.1

commit v2 on v1

v2 whole, which is shorter than its diff:
```python
import jax
import jax.numpy as jnp
from jax import lax
from jax.experimental import pallas as pl
from jax.experimental.pallas import tpu as pltpu
from jax.sharding import PartitionSpec as P

epsilon = 1e-06
LANES = 128
SUB = 8
NT = (((1,), (1,)), ((), ()))


def head_operands(raw, offset, h, half):
    lane = lax.broadcasted_iota(jnp.int32, raw.shape, 1)
    mine = (lane >= h * half) & (lane < (h + 1) * half)
    base = (1 - h) * half
    first = jnp.full(raw.shape, offset, jnp.float32)
    one = first.astype(jnp.bfloat16)
    rest = first - one.astype(jnp.float32)
    two = rest.astype(jnp.bfloat16)
    three = (rest - two.astype(jnp.float32)).astype(jnp.bfloat16)
    parts = jnp.where(lane == base, one, jnp.where(lane == base + 1, two, jnp.where(lane == base + 2, three, jnp.zeros_like(one))))
    return jnp.where(mine, raw, parts)


def key_operand(k, h, half):
    lane = lax.broadcasted_iota(jnp.int32, k.shape, 1)
    mine = (lane >= h * half) & (lane < (h + 1) * half)
    base = (1 - h) * half
    ones = jnp.where((lane >= base) & (lane < base + 3), jnp.ones_like(k), jnp.zeros_like(k))
    return jnp.where(mine, k, ones)


def suffix_products(total):
    row = lax.broadcasted_iota(jnp.int32, total.shape, 0)
    one = jnp.ones_like(total)

    def up(x, k):
        return jnp.where(row < SUB - k, pltpu.roll(x, SUB - k, 0), one)

    y = up(total, 1)
    y = y * up(y, 1)
    y = y * up(y, 2)
    return y * up(y, 4)


def tile_weights(halved, carry):
    keys, n = halved.shape
    steps = keys // SUB
    t = jnp.tanh(halved)
    take = 1.0 + t
    keep = 1.0 - t
    run = jnp.ones((SUB, n), jnp.float32)
    local = [None] * steps
    for v in reversed(range(steps)):
        local[v] = take[v * SUB : (v + 1) * SUB] * run
        run = run * keep[v * SUB : (v + 1) * SUB]
    total = run * (2.0 ** -steps)
    factor = suffix_products(total) * carry
    after = factor * total
    carry = jnp.broadcast_to(after[0:1], (SUB, n))
    return jnp.concatenate([x * factor for x in local], axis=0).astype(jnp.bfloat16), carry


MESH = pl.DeviceIdType.MESH
XN, ZN, YN = 4, 8, 4
ORDER = (1, 7, 2, 6, 3, 5, 4)


def pick(values, index):
    out = jnp.int32(values[0])
    for position, value in enumerate(values[1:], 1):
        out = jnp.where(index == position, jnp.int32(value), out)
    return out


def layer_kernel(
    off_ref, x_ref, gain_ref, wq_ref, wk_ref, wv_ref, wo_ref, ogain_ref, out_ref,
    xall, pm, pms, wvt, kbuf, vbuf, qbuf, qh, acc, carry, own_acc, own_keep, send_out, send_keep,
    ret_out, ret_keep, att, att_in, wo_all,
    x_send, x_recv, k_send, k_recv, v_send, v_recv, q_send, q_recv, ro_send, ro_recv, rk_send, rk_recv,
    a_send, a_recv, w_send, w_recv,
):
    sp, tp = lax.axis_index("sp"), lax.axis_index("tp")
    z, x = lax.div(sp, XN), lax.rem(sp, XN)
    y, c = lax.div(tp, 2), lax.rem(tp, 2)
    partner = (sp, y * 2 + 1 - c)
    rows, model = x_ref.shape
    chunks = YN * 2
    block = rows * chunks
    width = wq_ref.shape[1]
    half = width // 2
    steps = block // SUB

    def at_tp(other):
        return (sp, other)

    def at_x(other):
        return (z * XN + other, tp)

    def at_z(other):
        return (other * XN + x, tp)

    def copy(src, dst, ss, rs, device):
        return pltpu.make_async_remote_copy(src_ref=src, dst_ref=dst, send_sem=ss, recv_sem=rs, device_id=device, device_id_type=MESH)

    barrier = pltpu.get_barrier_semaphore()
    peers = [at_tp(lax.rem(tp + d, chunks)) for d in range(1, chunks)]
    peers += [at_x(lax.rem(x + d, XN)) for d in range(1, XN)]
    peers += [at_z(lax.rem(z + d, ZN)) for d in range(1, ZN)]
    for peer in peers:
        pl.semaphore_signal(barrier, inc=1, device_id=peer, device_id_type=MESH)
    wide = x_ref[...].astype(jnp.float32)
    spread = jnp.mean(wide * wide, axis=-1, keepdims=True)
    xall[tp] = (wide * lax.rsqrt(spread + epsilon) * gain_ref[...]).astype(jnp.bfloat16)
    pl.semaphore_wait(barrier, len(peers))

    def x_copy(chunk, slot, device):
        return copy(xall.at[chunk], xall.at[chunk], x_send.at[slot], x_recv.at[chunk], device)

    for d in (1, 3, 2):
        x_copy(tp, d - 1, at_tp(lax.rem(y + d, YN) * 2 + c)).start()
    x_copy(tp, 3, partner).start()

    row = lax.broadcasted_iota(jnp.int32, (block, block), 0)
    col = lax.broadcasted_iota(jnp.int32, (block, block), 1)
    token_of_row = lax.rem(row, SUB) * steps + lax.div(row, SUB)
    pm[...] = jnp.where(col == token_of_row, 1.0, 0.0).astype(jnp.bfloat16)
    token_of_col = lax.rem(col, SUB) * steps + lax.div(col, SUB)
    power = jnp.exp2((lax.div(col[0:1], SUB) - steps).astype(jnp.float32))
    pms[...] = jnp.where(row == token_of_col, power, 0.0).astype(jnp.bfloat16)
    wvt[...] = jnp.transpose(wv_ref[...])

    for d in (1, 3, 2):
        chunk = lax.rem(y + d, YN) * 2 + c
        x_copy(chunk, d - 1, partner).wait_recv()
        x_copy(chunk, 3 + d, partner).start()
    x_copy(y * 2 + 1 - c, 3, partner).wait_recv()
    for d in (1, 3, 2):
        x_copy(lax.rem(y + d, YN) * 2 + 1 - c, 3, partner).wait_recv()

    def w_copy(slot, d):
        return copy(wo_ref, wo_all.at[slot], w_send.at[d - 1], w_recv.at[slot], at_tp(lax.rem(tp + d, chunks)))

    normed = xall[...].reshape(block, model)
    q = jnp.dot(normed, wq_ref[...], preferred_element_type=jnp.float32).astype(jnp.bfloat16)
    qbuf[z] = q * jnp.bfloat16(0.0625)

    def q_copy(d):
        return copy(qbuf.at[z], qbuf.at[z], q_send.at[d - 1], q_recv.at[z], at_z(z - d))

    k = jnp.dot(normed, wk_ref[...], preferred_element_type=jnp.float32).astype(jnp.bfloat16)
    kbuf[x] = jnp.dot(pm[...], k, preferred_element_type=jnp.float32).astype(jnp.bfloat16)
    vt = lax.dot_general(wvt[...], normed, NT, preferred_element_type=jnp.float32).astype(jnp.bfloat16)
    vbuf[x] = jnp.dot(vt, pms[...], preferred_element_type=jnp.float32).astype(jnp.bfloat16)

    def k_copy(slot, d):
        return copy(kbuf.at[slot], kbuf.at[slot], k_send.at[d - 1], k_recv.at[slot], at_x(lax.rem(x + d, XN)))

    def v_copy(slot, d):
        return copy(vbuf.at[slot], vbuf.at[slot], v_send.at[d - 1], v_recv.at[slot], at_x(lax.rem(x + d, XN)))

    for d in (1, 3, 2):
        k_copy(x, d).start()
        v_copy(x, d).start()
    for d in ORDER:
        @pl.when(z >= d)
        def _():
            q_copy(d).start()
    for d in range(1, chunks):
        w_copy(tp, d).start()

    def prepare(slot):
        for h in range(2):
            qh[h] = head_operands(qbuf[slot], off_ref[h] * 0.5, h, half)
        acc[...] = jnp.zeros_like(acc)
        carry[...] = jnp.ones_like(carry)

    def tile(kb, h, diagonal):
        kh = key_operand(kbuf[kb], h, half)
        halved = lax.dot_general(kh, qh[h], NT, preferred_element_type=jnp.float32)
        if diagonal:
            query = lax.broadcasted_iota(jnp.int32, halved.shape, 1)
            row = lax.broadcasted_iota(jnp.int32, halved.shape, 0)
            halved = jnp.where(lax.rem(row, SUB) * steps + lax.div(row, SUB) < query, halved, -1e9)
        weights, carry[h] = tile_weights(halved, carry[h])
        acc[h * half : (h + 1) * half] += jnp.dot(vbuf[kb, h * half : (h + 1) * half], weights, preferred_element_type=jnp.float32)

    def tiles_down_from(first):
        def step(i, s):
            for h in range(2):
                tile(first - i, h, False)
            return s

        lax.fori_loop(0, first + 1, step, 0)

    prepare(z)
    for h in range(2):
        tile(x, h, True)
    for d in range(1, XN):
        other = lax.rem(x + d, XN)
        k_copy(other, 1).wait_recv()
        v_copy(other, 1).wait_recv()
    tiles_down_from(x - 1)
    own_acc[...] = acc[...]
    for h in range(2):
        own_keep[h : h + 1] = carry[h, 0:1]

    def out_copy(s, z_to):
        return copy(send_out.at[s], ret_out.at[z], ro_send.at[s], ro_recv.at[z], at_z(z_to))

    def keep_copy(s, z_to):
        return copy(send_keep.at[s], ret_keep.at[z], rk_send.at[s], rk_recv.at[z], at_z(z_to))

    def later(s, t):
        source = z + pick(ORDER, s)

        @pl.when(source < ZN)
        def _():
            copy(qbuf.at[source], qbuf.at[source], q_send.at[0], q_recv.at[source], partner).wait_recv()
            prepare(source)
            tiles_down_from(jnp.int32(XN - 1))
            send_out[s] = acc[...].astype(jnp.bfloat16)
            for h in range(2):
                send_keep[s, h : h + 1] = carry[h, 0:1]
            out_copy(s, source).start()
            keep_copy(s, source).start()

        return t

    lax.fori_loop(0, ZN - 1, later, 0)

    acc[...] = jnp.zeros_like(acc)

    def earlier(source, t):
        copy(ret_out.at[source], ret_out.at[source], ro_send.at[0], ro_recv.at[source], partner).wait_recv()
        copy(ret_keep.at[source], ret_keep.at[source], rk_send.at[0], rk_recv.at[source], partner).wait_recv()
        for h in range(2):
            part = slice(h * half, (h + 1) * half)
            acc[part] = acc[part] * ret_keep[source, h : h + 1] + ret_out[source, part].astype(jnp.float32)
        return t

    lax.fori_loop(0, z, earlier, 0)
    for h in range(2):
        part = slice(h * half, (h + 1) * half)
        acc[part] = acc[part] * own_keep[h : h + 1] + own_acc[part]
    att[...] = jnp.transpose(acc[...]).astype(jnp.bfloat16).reshape(att.shape)

    def a_copy(d):
        other = lax.rem(tp + d, chunks)
        return copy(att.at[other], att_in.at[tp], a_send.at[d - 1], a_recv.at[tp], at_tp(other))

    for d in range(1, chunks):
        a_copy(d).start()
    total = jnp.dot(att[tp], wo_ref[...], preferred_element_type=jnp.float32)
    for d in range(1, chunks):
        other = lax.rem(tp + d, chunks)
        w_copy(other, d).wait_recv()
        copy(att_in.at[other], att_in.at[other], a_send.at[0], a_recv.at[other], partner).wait_recv()
        total = total + jnp.dot(att_in[other], wo_all[other], preferred_element_type=jnp.float32)
    spread = jnp.mean(total * total, axis=-1, keepdims=True)
    out_ref[...] = (total * lax.rsqrt(spread + epsilon) * ogain_ref[...]).astype(jnp.bfloat16)

    for slot in range(chunks - 1):
        x_copy(tp, slot, partner).wait_send()
    for d in range(1, XN):
        k_copy(x, d).wait_send()
        v_copy(x, d).wait_send()
    for d in ORDER:
        @pl.when(z >= d)
        def _():
            q_copy(d).wait_send()
    for d in range(1, chunks):
        w_copy(tp, d).wait_send()
        a_copy(d).wait_send()

    def sent(s, t):
        @pl.when(z + pick(ORDER, s) < ZN)
        def _():
            out_copy(s, z).wait_send()
            keep_copy(s, z).wait_send()

        return t

    lax.fori_loop(0, ZN - 1, sent, 0)


def local(activations, input_gain, query_weight, key_weight, value_weight, stop_offset, output_weight, output_gain):
    rows, model = activations.shape
    width = query_weight.shape[1]
    chunks = lax.axis_size("tp")
    block = rows * chunks
    bf, f32, dma = jnp.bfloat16, jnp.float32, pltpu.SemaphoreType.DMA
    vmem = pl.BlockSpec(memory_space=pltpu.VMEM)
    return pl.pallas_call(
        layer_kernel,
        out_shape=jax.ShapeDtypeStruct((rows, model), bf),
        in_specs=[pl.BlockSpec(memory_space=pltpu.SMEM)] + [vmem] * 7,
        out_specs=vmem,
        scratch_shapes=[
            pltpu.VMEM((chunks, rows, model), bf),
            pltpu.VMEM((block, block), bf),
            pltpu.VMEM((block, block), bf),
            pltpu.VMEM((width, model), bf),
            pltpu.VMEM((XN, block, width), bf),
            pltpu.VMEM((XN, width, block), bf),
            pltpu.VMEM((ZN, block, width), bf),
            pltpu.VMEM((2, block, width), bf),
            pltpu.VMEM((width, block), f32),
            pltpu.VMEM((2, SUB, block), f32),
            pltpu.VMEM((width, block), f32),
            pltpu.VMEM((2, block), f32),
            pltpu.VMEM((ZN - 1, width, block), bf),
            pltpu.VMEM((ZN - 1, 2, block), f32),
            pltpu.VMEM((ZN, width, block), bf),
            pltpu.VMEM((ZN, 2, block), f32),
            pltpu.VMEM((chunks, rows, width), bf),
            pltpu.VMEM((chunks, rows, width), bf),
            pltpu.VMEM((chunks, width, model), bf),
            dma((7,)), dma((chunks,)),
            dma((3,)), dma((XN,)), dma((3,)), dma((XN,)),
            dma((7,)), dma((ZN,)),
            dma((7,)), dma((ZN,)), dma((7,)), dma((ZN,)),
            dma((7,)), dma((chunks,)), dma((7,)), dma((chunks,)),
        ],
        compiler_params=pltpu.CompilerParams(collective_id=0, has_side_effects=True, vmem_limit_bytes=56 * 1024 * 1024),
    )(stop_offset, activations, input_gain[None], query_weight, key_weight, value_weight, output_weight, output_gain[None])


def solution(mesh):
    in_specs = (P(("sp", "tp"), None), P(), P(None, "tp"), P(None, "tp"), P(None, "tp"), P("tp"), P("tp", None), P())
    return jax.shard_map(local, mesh=mesh, in_specs=in_specs, out_specs=P(("sp", "tp"), None), check_vma=False)
```

time: 292 us -> 81.9 us (0.28)
  the two profiles are of different devices: /device:TPU:231 before, /device:TPU:167 now
where the time goes in v2:
time: 81.9 us; the launch traced here: 81.8 us
  Pallas kernels  80.2 us (98%)
  local copies, waits for them, and re-layouts  1.57 us (2%)
    pallas_call x1, Pallas kernels, local(): pl.pallas_call(layer_kernel, out_shape=jax.ShapeDtypeStruct((rows, model)...  80.2 us

profile of v2, /device:TPU:167, one launch (start us, length us, event | category | flops | bytes accessed | tf_op | source)
XLA Modules:
  0.0 81.8 jit_solution(8484130516443955569)
XLA Ops:
  0.0 80.2 %shard_map.82 = bf16[64,1024]{1,0:T(8,128)(2,1)} custom-call(f32[2]{0:T(128)} %off_ref.1, bf16[64,1024]{1,0:T(8,128)(2,1)} %x_ref.1, f32[1,1024]{1,0:T(1,128)} %bitcast.2, bf16[1024,128]{1,0:T(8,128)(2,1)} %wq_ref.1, bf16[1024,128]{1,0:T(8,128)(2,1)} %wk_ref.1, bf16[1024,128]{1,0:T(8,128)(2,1)} %wv_ref.1, bf16[128,1024]{1,0:T(8,128)(2,1)} %wo_ref.1, ...), custom_call_target="tpu_custom_call" | custom-call | tf_op jit(solution)/shard_map/pallas_call | solution.py:296
  80.2 1.6 %copy.10 = bf16[64,1024]{1,0:T(8,128)(2,1)} copy(bf16[64,1024]{1,0:T(8,128)(2,1)} %shard_map.82) | data formatting | bytes 262144

commit v3 on v1

v3 whole, which is shorter than its diff:
```python
import jax
import jax.numpy as jnp
from jax import lax
from jax.experimental import pallas as pl
from jax.experimental.pallas import tpu as pltpu
from jax.sharding import PartitionSpec as P

epsilon = 1e-06
SUB = 8
NT = (((1,), (1,)), ((), ()))
MESH = pl.DeviceIdType.MESH
XN, ZN, YN = 4, 8, 4
LAST = ZN - 1
Q_ORDER = (7, 6, 1, 5, 2, 4, 3)


def suffix_products(total):
    row = lax.broadcasted_iota(jnp.int32, total.shape, 0)

    def up(a, k):
        return jnp.where(row < SUB - k, pltpu.roll(a, SUB - k, 0), 1.0)

    y = up(total, 1)
    y = y * up(y, 1)
    y = y * up(y, 2)
    return y * up(y, 4)


def tile_weights(halved, carry, w_ref):
    keys, n = halved.shape
    steps = keys // SUB
    run = jnp.ones((SUB, n), jnp.float32)
    local = []
    for v in range(steps):
        part = run * jnp.tanh(halved[v * SUB : (v + 1) * SUB])
        local.append(run + part)
        run = run - part
    total = run * (2.0**-steps)
    factor = suffix_products(total) * carry
    for u in range(steps // 2):
        pair = jnp.concatenate([local[2 * u] * factor, local[2 * u + 1] * factor], axis=0)
        w_ref[2 * SUB * u : 2 * SUB * (u + 1)] = pair.astype(jnp.bfloat16)
    return jnp.broadcast_to((factor * total)[0:1], (SUB, n))


def layer_kernel(
    off_ref, x_ref, gain_ref, wq_ref, wk_ref, wv_ref, wo_ref, ogain_ref, out_ref,
    xall, wt, pk, pv_, qmine, kmate, vmate, qbuf, kt, vt, kop, qop, wa, wb, wc, wd, acc, carry,
    send_out, send_keep, ret_out, ret_keep, att, att_in, wo_all,
    x_send, x_recv, xh_recv, m_send, k_send, k_recv, v_send, v_recv, q_send, q_recv,
    ro_send, ro_recv, rk_send, rk_recv, a_send, a_recv, w_send, w_recv,
):
    sp, tp = lax.axis_index("sp"), lax.axis_index("tp")
    z, x = lax.div(sp, XN), lax.rem(sp, XN)
    y, c = lax.div(tp, 2), lax.rem(tp, 2)
    mate = LAST - z
    head = lax.div(z, ZN // 2)
    other = 1 - head
    partner = (sp, y * 2 + 1 - c)
    rows, model = x_ref.shape
    chunks = YN * 2
    block = rows * chunks
    width = wq_ref.shape[1]
    half = width // 2
    steps = block // SUB
    bf, f32 = jnp.bfloat16, jnp.float32

    def at_tp(o):
        return (sp, o)

    def at_x(o):
        return (z * XN + o, tp)

    def at_z(o):
        return (o * XN + x, tp)

    def copy(src, dst, ss, rs, device):
        return pltpu.make_async_remote_copy(src_ref=src, dst_ref=dst, send_sem=ss, recv_sem=rs, device_id=device, device_id_type=MESH)

    def along_y(d):
        return lax.rem(y + d, YN)

    def along_x(d):
        return lax.rem(x + d, XN)

    barrier = pltpu.get_barrier_semaphore()
    peers = [at_tp(lax.rem(tp + d, chunks)) for d in range(1, chunks)]
    peers += [at_x(along_x(1)), at_x(along_x(XN - 1))]
    peers += [at_z(lax.rem(z + d, ZN)) for d in range(1, ZN)]
    for peer in peers:
        pl.semaphore_signal(barrier, inc=1, device_id=peer, device_id_type=MESH)
    wide = x_ref[...].astype(f32)
    spread = jnp.mean(wide * wide, axis=-1, keepdims=True)
    xall[tp] = (wide * lax.rsqrt(spread + epsilon) * gain_ref[...]).astype(bf).reshape(xall.shape[1:])
    pl.semaphore_wait(barrier, len(peers))

    def x_full(chunk, slot, device):
        return copy(xall.at[chunk], xall.at[chunk], x_send.at[slot], x_recv.at[chunk], device)

    def x_half(chunk, part, slot, side, device):
        return copy(xall.at[chunk, part], xall.at[chunk, part], x_send.at[slot], xh_recv.at[side, part], device)

    def same(d):
        return along_y(d) * 2 + c

    def across(d):
        return along_y(d) * 2 + 1 - c

    x_full(tp, 0, at_tp(same(1))).start()
    x_full(tp, 1, at_tp(same(3))).start()
    x_full(tp, 2, partner).start()

    row = lax.broadcasted_iota(jnp.int32, (block, block), 0)
    col = lax.broadcasted_iota(jnp.int32, (1, block), 1)
    step_of = lax.div(col, SUB)
    hit = row == lax.rem(col, SUB) * steps + (steps - 1) - step_of
    pk[...] = jnp.where(hit, 1.0, 0.0).astype(bf)
    pv_[...] = jnp.where(hit, jnp.exp2(-(step_of + 1).astype(f32)), 0.0).astype(bf)
    wt[0] = jnp.transpose(wq_ref[...])
    wt[1] = jnp.transpose(wk_ref[...])
    wt[2] = jnp.transpose(wv_ref[...])
    low = lax.broadcasted_iota(jnp.int32, (half, block), 0)
    first = jnp.full((half, block), off_ref[head] * 0.5, f32)
    one = first.astype(bf)
    rest = first - one.astype(f32)
    two = rest.astype(bf)
    three = (rest - two.astype(f32)).astype(bf)
    qop[half:] = jnp.where(low == 0, one, jnp.where(low == 1, two, jnp.where(low == 2, three, jnp.zeros_like(one))))
    ones = jnp.where(low < 3, 1.0, 0.0).astype(bf)

    x_full(same(3), 0, partner).wait_recv()
    x_half(same(3), 0, 3, 0, at_tp(same(1))).start()
    x_full(same(3), 4, partner).start()
    x_full(same(1), 0, partner).wait_recv()
    x_half(same(1), 1, 5, 0, at_tp(same(3))).start()
    x_full(same(1), 6, partner).start()
    for part in range(2):
        x_half(same(2), part, 0, 0, partner).wait_recv()
        x_half(same(2), part, 7 + part, 1, partner).start()
    for d in (0, 1, 3):
        x_full(across(d), 0, partner).wait_recv()
    for part in range(2):
        x_half(across(2), part, 0, 1, partner).wait_recv()

    normed = xall[...].reshape(block, model)
    projected = lax.dot_general(wt[...].reshape(3 * width, model), normed, NT, preferred_element_type=f32).astype(bf)
    q_all = projected[0:width] * bf(0.0625)
    k_all = jnp.dot(projected[width : 2 * width], pk[...], preferred_element_type=f32).astype(bf)
    v_all = jnp.dot(projected[2 * width :], pv_[...], preferred_element_type=f32).astype(bf)
    qmine[...] = q_all.reshape(qmine.shape)
    k_two = k_all.reshape(2, half, block)
    v_two = v_all.reshape(2, half, block)
    upper = head == 1
    kt[head, x] = jnp.where(upper, k_two[1], k_two[0])
    vt[head, x] = jnp.where(upper, v_two[1], v_two[0])
    kmate[...] = jnp.where(upper, k_two[0], k_two[1])
    vmate[...] = jnp.where(upper, v_two[0], v_two[1])

    def k_copy(slab, chunk, slot, device):
        return copy(kt.at[slab, chunk], kt.at[slab, chunk], k_send.at[slab, slot], k_recv.at[slab, chunk], device)

    def v_copy(slab, chunk, slot, device):
        return copy(vt.at[slab, chunk], vt.at[slab, chunk], v_send.at[slab, slot], v_recv.at[slab, chunk], device)

    def mate_copies():
        return (
            copy(kmate, kt.at[head, x], m_send.at[0], k_recv.at[head, x], at_z(mate)),
            copy(vmate, vt.at[head, x], m_send.at[1], v_recv.at[head, x], at_z(mate)),
        )

    def spread_block(slab):
        for slot, d in ((0, 1), (1, XN - 1)):
            k_copy(slab, x, slot, at_x(along_x(d))).start()
            v_copy(slab, x, slot, at_x(along_x(d))).start()

    def pass_on(slab):
        left, right = along_x(XN - 1), along_x(1)
        k_copy(slab, left, 0, partner).wait_recv()
        k_copy(slab, left, 2, at_x(right)).start()
        v_copy(slab, right, 0, partner).wait_recv()
        v_copy(slab, right, 2, at_x(left)).start()
        v_copy(slab, left, 0, partner).wait_recv()
        k_copy(slab, right, 0, partner).wait_recv()

    def opposite(slab):
        far = along_x(2)
        k_copy(slab, far, 0, partner).wait_recv()
        v_copy(slab, far, 0, partner).wait_recv()

    def key_rows(slab, chunk):
        kop[slab, chunk] = jnp.transpose(jnp.concatenate([kt[slab, chunk], ones], axis=0))

    for sent in mate_copies():
        sent.start()
    spread_block(head)

    def target(d):
        return lax.rem(z + d, ZN)

    def reaches(d):
        return jnp.minimum(target(d), LAST - target(d)) <= z

    def q_copy(d):
        return copy(qmine.at[lax.div(target(d), ZN // 2)], qbuf.at[z], q_send.at[d - 1], q_recv.at[z], at_z(target(d)))

    for d in Q_ORDER:
        @pl.when(reaches(d))
        def _():
            q_copy(d).start()

    def w_copy(slot, d):
        return copy(wo_ref, wo_all.at[slot], w_send.at[d - 1], w_recv.at[slot], at_tp(lax.rem(tp + d, chunks)))

    for d in range(1, chunks):
        w_copy(tp, d).start()

    def q_arrived(source):
        copy(qbuf.at[source], qbuf.at[source], q_send.at[0], q_recv.at[source], partner).wait_recv()

    def scores(slab, kb):
        return jnp.dot(kop[slab, kb], qop[...], preferred_element_type=f32)

    def values(slab, kb, w_ref):
        return jnp.dot(vt[slab, kb], w_ref[...], preferred_element_type=f32)

    def out_copy(slab, source):
        index = jnp.where(slab == head, z, mate)
        return (
            copy(send_out.at[slab, source], ret_out.at[index, head], ro_send.at[slab, source], ro_recv.at[index, head], at_z(source)),
            copy(send_keep.at[slab, source], ret_keep.at[index, head], rk_send.at[slab, source], rk_recv.at[index, head], at_z(source)),
        )

    def deliver(slab, source, part, keep):
        @pl.when(source == z)
        def _():
            index = jnp.where(slab == head, z, mate)
            ret_out[index, head] = part.astype(bf)
            ret_keep[index, head] = keep[0:1]

        @pl.when(source != z)
        def _():
            send_out[slab, source] = part.astype(bf)
            send_keep[slab, source] = keep[0:1]
            for sent in out_copy(slab, source):
                sent.start()

    def full_set(slab, source):
        qop[0:half] = qbuf[source]
        keep = jnp.ones((SUB, block), f32)
        keep = tile_weights(scores(slab, 3), keep, wa)
        keep = tile_weights(scores(slab, 2), keep, wb)
        part = values(slab, 3, wa)
        keep = tile_weights(scores(slab, 1), keep, wc)
        part = part + values(slab, 2, wb)
        keep = tile_weights(scores(slab, 0), keep, wd)
        part = part + values(slab, 1, wc)
        part = part + values(slab, 0, wd)
        deliver(slab, source, part, keep)

    def diagonal_tile(slab):
        halved = scores(slab, x)
        r = lax.broadcasted_iota(jnp.int32, halved.shape, 0)
        query = lax.broadcasted_iota(jnp.int32, halved.shape, 1)
        key = lax.rem(r, SUB) * steps + (steps - 1) - lax.div(r, SUB)
        halved = jnp.where(key < query, halved, -1e9)
        carry[...] = tile_weights(halved, jnp.ones((SUB, block), f32), wa)
        acc[0:half] = values(slab, x, wa)

    def below_diagonal(slab, source):
        def step(i, t):
            kb = x - 1 - i
            carry[...] = tile_weights(scores(slab, kb), carry[...], wa)
            acc[0:half] += values(slab, kb, wa)
            return t

        lax.fori_loop(0, x, step, 0)
        deliver(slab, source, acc[0:half], carry[...])

    qbuf[z] = qmine[head]
    qop[0:half] = qmine[head]
    key_rows(head, x)
    diagonal_tile(head)
    pass_on(head)
    k_copy(other, x, 0, partner).wait_recv()
    v_copy(other, x, 0, partner).wait_recv()
    spread_block(other)
    opposite(head)
    for d in range(1, XN):
        key_rows(head, along_x(d))
    below_diagonal(head, z)

    own_jobs = LAST - z

    def job(n, t):
        @pl.when(n == jnp.minimum(2, own_jobs))
        def _():
            pass_on(other)

        @pl.when(n == own_jobs)
        def _():
            opposite(other)
            for d in range(XN):
                key_rows(other, along_x(d))

        @pl.when(n < LAST)
        def _():
            mine = n < own_jobs
            slab = jnp.where(mine, head, other)
            source = jnp.where(mine, z + 1 + n, n + 1)

            @pl.when(mine | (source < z))
            def _():
                q_arrived(source)

            full_set(slab, source)

        return t

    lax.fori_loop(0, ZN, job, 0)

    @pl.when(upper)
    def _():
        q_arrived(mate)

    qop[0:half] = qbuf[mate]
    diagonal_tile(other)
    below_diagonal(other, mate)

    acc[...] = jnp.zeros_like(acc)

    def gather(slab, t):
        for h in range(2):
            low_z = jnp.minimum(slab, LAST - slab)
            provider = low_z if h == 0 else LAST - low_z

            @pl.when(provider != z)
            def _():
                copy(ret_out.at[slab, h], ret_out.at[slab, h], ro_send.at[0, 0], ro_recv.at[slab, h], partner).wait_recv()
                copy(ret_keep.at[slab, h], ret_keep.at[slab, h], rk_send.at[0, 0], rk_recv.at[slab, h], partner).wait_recv()

            span = slice(h * half, (h + 1) * half)
            acc[span] = acc[span] * ret_keep[slab, h] + ret_out[slab, h].astype(f32)
        return t

    lax.fori_loop(0, z + 1, gather, 0)
    att[...] = jnp.transpose(acc[...]).astype(bf).reshape(att.shape)

    def a_copy(d):
        o = lax.rem(tp + d, chunks)
        return copy(att.at[o], att_in.at[tp], a_send.at[d - 1], a_recv.at[tp], at_tp(o))

    for d in range(1, chunks):
        a_copy(d).start()
    total = jnp.dot(att[tp], wo_ref[...], preferred_element_type=f32)
    for d in range(1, chunks):
        o = lax.rem(tp + d, chunks)
        w_copy(o, d).wait_recv()
        copy(att_in.at[o], att_in.at[o], a_send.at[0], a_recv.at[o], partner).wait_recv()
        total = total + jnp.dot(att_in[o], wo_all[o], preferred_element_type=f32)
    spread = jnp.mean(total * total, axis=-1, keepdims=True)
    out_ref[...] = (total * lax.rsqrt(spread + epsilon) * ogain_ref[...]).astype(bf)

    for slot in (0, 1, 2, 4, 6):
        x_full(tp, slot, partner).wait_send()
    for slot in (3, 5, 7, 8):
        x_half(tp, 0, slot, 0, partner).wait_send()
    for sent in mate_copies():
        sent.wait_send()
    for slab in range(2):
        for slot in range(3):
            k_copy(slab, x, slot, partner).wait_send()
            v_copy(slab, x, slot, partner).wait_send()
    for d in Q_ORDER:
        @pl.when(reaches(d))
        def _():
            q_copy(d).wait_send()
    for d in range(1, chunks):
        w_copy(tp, d).wait_send()
        a_copy(d).wait_send()

    def drained(source, t):
        @pl.when((source >= z) & (source != z))
        def _():
            for sent in out_copy(head, source):
                sent.wait_send()

        @pl.when((source >= mate) & (source != z))
        def _():
            for sent in out_copy(other, source):
                sent.wait_send()

        return t

    lax.fori_loop(0, ZN, drained, 0)


def local(activations, input_gain, query_weight, key_weight, value_weight, stop_offset, output_weight, output_gain):
    rows, model = activations.shape
    width = query_weight.shape[1]
    half = width // 2
    chunks = lax.axis_size("tp")
    block = rows * chunks
    bf, f32, dma = jnp.bfloat16, jnp.float32, pltpu.SemaphoreType.DMA
    vmem = pl.BlockSpec(memory_space=pltpu.VMEM)
    return pl.pallas_call(
        layer_kernel,
        out_shape=jax.ShapeDtypeStruct((rows, model), bf),
        in_specs=[pl.BlockSpec(memory_space=pltpu.SMEM)] + [vmem] * 7,
        out_specs=vmem,
        scratch_shapes=[
            pltpu.VMEM((chunks, 2, rows // 2, model), bf),
            pltpu.VMEM((3, width, model), bf),
            pltpu.VMEM((block, block), bf),
            pltpu.VMEM((block, block), bf),
            pltpu.VMEM((2, half, block), bf),
            pltpu.VMEM((half, block), bf),
            pltpu.VMEM((half, block), bf),
            pltpu.VMEM((ZN, half, block), bf),
            pltpu.VMEM((2, XN, half, block), bf),
            pltpu.VMEM((2, XN, half, block), bf),
            pltpu.VMEM((2, XN, block, width), bf),
            pltpu.VMEM((width, block), bf),
            *[pltpu.VMEM((block, block), bf)] * 4,
            pltpu.VMEM((width, block), f32),
            pltpu.VMEM((SUB, block), f32),
            pltpu.VMEM((2, ZN, half, block), bf),
            pltpu.VMEM((2, ZN, 1, block), f32),
            pltpu.VMEM((ZN, 2, half, block), bf),
            pltpu.VMEM((ZN, 2, 1, block), f32),
            pltpu.VMEM((chunks, rows, width), bf),
            pltpu.VMEM((chunks, rows, width), bf),
            pltpu.VMEM((chunks, width, model), bf),
            dma((9,)), dma((chunks,)), dma((2, 2)), dma((2,)),
            dma((2, 3)), dma((2, XN)), dma((2, 3)), dma((2, XN)),
            dma((7,)), dma((ZN,)),
            dma((2, ZN)), dma((ZN, 2)), dma((2, ZN)), dma((ZN, 2)),
            dma((7,)), dma((chunks,)), dma((7,)), dma((chunks,)),
        ],
        compiler_params=pltpu.CompilerParams(collective_id=0, has_side_effects=True, vmem_limit_bytes=56 * 1024 * 1024),
    )(stop_offset, activations, input_gain[None], query_weight, key_weight, value_weight, output_weight, output_gain[None])


def solution(mesh):
    in_specs = (P(("sp", "tp"), None), P(), P(None, "tp"), P(None, "tp"), P(None, "tp"), P("tp"), P("tp", None), P())
    return jax.shard_map(local, mesh=mesh, in_specs=in_specs, out_specs=P(("sp", "tp"), None), check_vma=False)
```

time: 292 us -> 65.5 us (0.22); the launches traced: 287 us -> 65.4 us
  waiting for transfers between devices: 210 us -> 0 us
  Pallas kernels: 40.7 us -> 63.8 us
  between operations: 13.2 us -> 0.01 us
  local copies, waits for them, and re-layouts: 9.59 us -> 1.57 us
  matrix products: 6.45 us -> 0 us
  other arithmetic: 6.27 us -> 0 us
    all_gather x3 -> x0, waiting for transfers between devices: 176 us -> none  [the longest x1 76.3 us: local(): kp = lax.all_gather(kp, 'sp', axis=0, tiled=False)]
    reduce_scatter x1 -> x0, waiting for transfers between devices: 34.6 us -> none  [local(): lax.psum_scatter(out, 'tp', scatter_dimension=0, tiled=True)]
    pallas_call x1, Pallas kernels: 40.7 us -> 63.8 us  [local(): pl.pallas_call(layer_kernel, out_shape=jax.ShapeDtypeStruct((rows, model)...]
    all_gather x1 -> x0, local copies, waits for them, and re-layouts: 6.46 us -> none  [local(): vt = lax.all_gather(vt, 'sp', axis=0, tiled=False)]
    dot_general x4 -> x0, matrix products: 6.45 us -> none  [the longest x3 5.06 us: proj(): jnp.dot(whole, w, preferred_element_type=jnp.float32).astype(jnp.bfloat16)]
    convert_element_type x3 -> x0, other arithmetic: 3.34 us -> none  [the longest x2 3.33 us: scaled_rows(): (widened * lax.rsqrt(spread + epsilon) * row_gain).astype(jnp.bfloat16)]
  transfers between devices with their start and end apart: 4 -> 0, of which waited for: 4 -> 0; matrix products, arithmetic and copies ran while one was open for 4% -> 0% of each run, Pallas kernels for 0% -> 0%
where the time goes in v3:
time: 65.5 us; the launch traced here: 65.4 us
  Pallas kernels  63.8 us (97%)
  local copies, waits for them, and re-layouts  1.57 us (2%)
    pallas_call x1, Pallas kernels, local(): pl.pallas_call(layer_kernel, out_shape=jax.ShapeDtypeStruct((rows, model)...  63.8 us
    unnamed x1, local copies, waits for them, and re-layouts  1.57 us

profile of v3, /device:TPU:231, one launch (start us, length us, event | category | flops | bytes accessed | tf_op | source)
XLA Modules:
  0.0 65.4 jit_solution(8630945662545306648)
XLA Ops:
  0.0 63.8 %shard_map.82 = bf16[64,1024]{1,0:T(8,128)(2,1)} custom-call(f32[2]{0:T(128)} %off_ref.1, bf16[64,1024]{1,0:T(8,128)(2,1)} %x_ref.1, f32[1,1024]{1,0:T(1,128)} %bitcast.2, bf16[1024,128]{1,0:T(8,128)(2,1)} %wq_ref.1, bf16[1024,128]{1,0:T(8,128)(2,1)} %wk_ref.1, bf16[1024,128]{1,0:T(8,128)(2,1)} %wv_ref.1, bf16[128,1024]{1,0:T(8,128)(2,1)} %wo_ref.1, ...), custom_call_target="tpu_custom_call" | custom-call | tf_op jit(solution)/shard_map/pallas_call | solution.py:405
  63.8 1.6 %copy.10 = bf16[64,1024]{1,0:T(8,128)(2,1)} copy(bf16[64,1024]{1,0:T(8,128)(2,1)} %shard_map.82) | data formatting | bytes 262144

commit v4 on v3

--- a/solution.py
+++ b/solution.py
@@ -47,7 +47,7 @@
     off_ref, x_ref, gain_ref, wq_ref, wk_ref, wv_ref, wo_ref, ogain_ref, out_ref,
     xall, wt, pk, pv_, qmine, kmate, vmate, qbuf, kt, vt, kop, qop, wa, wb, wc, wd, acc, carry,
     send_out, send_keep, ret_out, ret_keep, att, att_in, wo_all,
-    x_send, x_recv, xh_recv, m_send, k_send, k_recv, v_send, v_recv, q_send, q_recv,
+    x_send, x_recv, m_send, k_send, k_recv, v_send, v_recv, q_send, q_recv,
     ro_send, ro_recv, rk_send, rk_recv, a_send, a_recv, w_send, w_recv,
 ):
     sp, tp = lax.axis_index("sp"), lax.axis_index("tp")
@@ -94,21 +94,56 @@
     xall[tp] = (wide * lax.rsqrt(spread + epsilon) * gain_ref[...]).astype(bf).reshape(xall.shape[1:])
     pl.semaphore_wait(barrier, len(peers))
 
-    def x_full(chunk, slot, device):
-        return copy(xall.at[chunk], xall.at[chunk], x_send.at[slot], x_recv.at[chunk], device)
-
-    def x_half(chunk, part, slot, side, device):
-        return copy(xall.at[chunk, part], xall.at[chunk, part], x_send.at[slot], xh_recv.at[side, part], device)
-
     def same(d):
         return along_y(d) * 2 + c
 
     def across(d):
         return along_y(d) * 2 + 1 - c
 
-    x_full(tp, 0, at_tp(same(1))).start()
-    x_full(tp, 1, at_tp(same(3))).start()
-    x_full(tp, 2, partner).start()
+    class TpGather:
+        def __init__(self, buf, send, recv):
+            self.buf, self.send, self.recv = buf, send, recv
+
+        def part(self, chunk, h, slot, device):
+            piece = self.buf.at[chunk, h]
+            return copy(piece, piece, self.send.at[slot], self.recv.at[chunk, h], device)
+
+        def begin(self):
+            for slot, (h, device) in enumerate(((0, same(1)), (1, same(3)), (1, same(1)), (0, same(3)))):
+                self.part(tp, h, slot, at_tp(device)).start()
+            for h in range(2):
+                self.part(tp, h, 4 + h, partner).start()
+
+        def take(self, chunk, h, slot):
+            self.part(chunk, h, 0, partner).wait_recv()
+            if slot is not None:
+                self.part(chunk, h, slot, partner).start()
+
+        def relay(self):
+            self.take(same(3), 0, 6)
+            self.part(same(3), 0, 12, at_tp(same(1))).start()
+            self.take(same(1), 1, 7)
+            self.part(same(1), 1, 13, at_tp(same(3))).start()
+            self.take(same(3), 1, 8)
+            self.take(same(1), 0, 9)
+
+        def relay_far(self):
+            self.take(same(2), 0, 10)
+            self.take(same(2), 1, 11)
+
+        def complete(self):
+            for d in (0, 1, 3, 2):
+                for h in range(2):
+                    self.take(across(d), h, None)
+
+        def drain(self):
+            for slot in range(14):
+                self.part(tp, 0, slot, partner).wait_send()
+
+    x_gather = TpGather(xall, x_send, x_recv)
+    w_gather = TpGather(wo_all, w_send, w_recv)
+    x_gather.begin()
+    wo_all[tp] = wo_ref[...].reshape(wo_all.shape[1:])
 
     row = lax.broadcasted_iota(jnp.int32, (block, block), 0)
     col = lax.broadcasted_iota(jnp.int32, (1, block), 1)
@@ -128,19 +163,9 @@
     qop[half:] = jnp.where(low == 0, one, jnp.where(low == 1, two, jnp.where(low == 2, three, jnp.zeros_like(one))))
     ones = jnp.where(low < 3, 1.0, 0.0).astype(bf)
 
-    x_full(same(3), 0, partner).wait_recv()
-    x_half(same(3), 0, 3, 0, at_tp(same(1))).start()
-    x_full(same(3), 4, partner).start()
-    x_full(same(1), 0, partner).wait_recv()
-    x_half(same(1), 1, 5, 0, at_tp(same(3))).start()
-    x_full(same(1), 6, partner).start()
-    for part in range(2):
-        x_half(same(2), part, 0, 0, partner).wait_recv()
-        x_half(same(2), part, 7 + part, 1, partner).start()
-    for d in (0, 1, 3):
-        x_full(across(d), 0, partner).wait_recv()
-    for part in range(2):
-        x_half(across(2), part, 0, 1, partner).wait_recv()
+    x_gather.relay()
+    x_gather.relay_far()
+    x_gather.complete()
 
     normed = xall[...].reshape(block, model)
     projected = lax.dot_general(wt[...].reshape(3 * width, model), normed, NT, preferred_element_type=f32).astype(bf)
@@ -168,17 +193,23 @@
             copy(vmate, vt.at[head, x], m_send.at[1], v_recv.at[head, x], at_z(mate)),
         )
 
-    def spread_block(slab):
+    def spread_keys(slab):
         for slot, d in ((0, 1), (1, XN - 1)):
             k_copy(slab, x, slot, at_x(along_x(d))).start()
+
+    def spread_values(slab):
+        for slot, d in ((0, XN - 1), (1, 1)):
             v_copy(slab, x, slot, at_x(along_x(d))).start()
 
+    left, right = along_x(XN - 1), along_x(1)
+
     def pass_on(slab):
-        left, right = along_x(XN - 1), along_x(1)
         k_copy(slab, left, 0, partner).wait_recv()
         k_copy(slab, left, 2, at_x(right)).start()
         v_copy(slab, right, 0, partner).wait_recv()
         v_copy(slab, right, 2, at_x(left)).start()
+
+    def beside(slab):
         v_copy(slab, left, 0, partner).wait_recv()
         k_copy(slab, right, 0, partner).wait_recv()
 
@@ -192,7 +223,8 @@
 
     for sent in mate_copies():
         sent.start()
-    spread_block(head)
+    spread_keys(head)
+    spread_values(head)
 
     def target(d):
         return lax.rem(z + d, ZN)
@@ -208,11 +240,7 @@
         def _():
             q_copy(d).start()
 
-    def w_copy(slot, d):
-        return copy(wo_ref, wo_all.at[slot], w_send.at[d - 1], w_recv.at[slot], at_tp(lax.rem(tp + d, chunks)))
-
-    for d in range(1, chunks):
-        w_copy(tp, d).start()
+    w_gather.begin()
 
     def q_arrived(source):
         copy(qbuf.at[source], qbuf.at[source], q_send.at[0], q_recv.at[source], partner).wait_recv()
@@ -223,24 +251,48 @@
     def values(slab, kb, w_ref):
         return jnp.dot(vt[slab, kb], w_ref[...], preferred_element_type=f32)
 
+    centre = (z == ZN // 2 - 1) | (z == ZN // 2)
+
+    def joined(source):
+        return centre & (source >= ZN // 2)
+
+    def slab_index(slab, source):
+        return jnp.where(joined(source), ZN // 2, jnp.where(slab == head, z, mate))
+
     def out_copy(slab, source):
-        index = jnp.where(slab == head, z, mate)
+        index = slab_index(slab, source)
         return (
             copy(send_out.at[slab, source], ret_out.at[index, head], ro_send.at[slab, source], ro_recv.at[index, head], at_z(source)),
             copy(send_keep.at[slab, source], ret_keep.at[index, head], rk_send.at[slab, source], rk_recv.at[index, head], at_z(source)),
         )
 
     def deliver(slab, source, part, keep):
-        @pl.when(source == z)
-        def _():
-            index = jnp.where(slab == head, z, mate)
-            ret_out[index, head] = part.astype(bf)
-            ret_keep[index, head] = keep[0:1]
-
-        @pl.when(source != z)
-        def _():
-            send_out[slab, source] = part.astype(bf)
-            send_keep[slab, source] = keep[0:1]
+        acc[0:half] = part
+        carry[...] = keep
+
+        @pl.when(joined(source) & (slab == other))
+        def _():
+            before, kept = send_out[head, source].astype(f32), send_keep[head, source]
+            now = acc[0:half]
+            first, second = jnp.where(upper, before, now), jnp.where(upper, now, before)
+            acc[0:half] = first + jnp.where(upper, kept, carry[0:1]) * second
+            carry[0:1] = carry[0:1] * kept
+
+        waits = joined(source) & (slab == head)
+
+        @pl.when((source == z) & jnp.logical_not(waits))
+        def _():
+            index = slab_index(slab, source)
+            ret_out[index, head] = acc[0:half].astype(bf)
+            ret_keep[index, head] = carry[0:1]
+
+        @pl.when((source != z) | waits)
+        def _():
+            send_out[slab, source] = acc[0:half].astype(bf)
+            send_keep[slab, source] = carry[0:1]
+
+        @pl.when((source != z) & jnp.logical_not(waits))
+        def _():
             for sent in out_copy(slab, source):
                 sent.start()
 
@@ -282,9 +334,12 @@
     diagonal_tile(head)
     pass_on(head)
     k_copy(other, x, 0, partner).wait_recv()
+    spread_keys(other)
     v_copy(other, x, 0, partner).wait_recv()
-    spread_block(other)
+    spread_values(other)
+    beside(head)
     opposite(head)
+    w_gather.relay()
     for d in range(1, XN):
         key_rows(head, along_x(d))
     below_diagonal(head, z)
@@ -296,8 +351,13 @@
         def _():
             pass_on(other)
 
+        @pl.when(n == 3)
+        def _():
+            w_gather.relay_far()
+
         @pl.when(n == own_jobs)
         def _():
+            beside(other)
             opposite(other)
             for d in range(XN):
                 key_rows(other, along_x(d))
@@ -332,14 +392,18 @@
         for h in range(2):
             low_z = jnp.minimum(slab, LAST - slab)
             provider = low_z if h == 0 else LAST - low_z
-
-            @pl.when(provider != z)
+            held = (slab != ZN // 2 - 1) | (z < ZN // 2)
+
+            @pl.when(held & (provider != z))
             def _():
                 copy(ret_out.at[slab, h], ret_out.at[slab, h], ro_send.at[0, 0], ro_recv.at[slab, h], partner).wait_recv()
                 copy(ret_keep.at[slab, h], ret_keep.at[slab, h], rk_send.at[0, 0], rk_recv.at[slab, h], partner).wait_recv()
 
-            span = slice(h * half, (h + 1) * half)
-            acc[span] = acc[span] * ret_keep[slab, h] + ret_out[slab, h].astype(f32)
+            @pl.when(held)
+            def _():
+                span = slice(h * half, (h + 1) * half)
+                acc[span] = acc[span] * ret_keep[slab, h] + ret_out[slab, h].astype(f32)
+
         return t
 
     lax.fori_loop(0, z + 1, gather, 0)
@@ -352,18 +416,16 @@
     for d in range(1, chunks):
         a_copy(d).start()
     total = jnp.dot(att[tp], wo_ref[...], preferred_element_type=f32)
+    w_gather.complete()
     for d in range(1, chunks):
         o = lax.rem(tp + d, chunks)
-        w_copy(o, d).wait_recv()
         copy(att_in.at[o], att_in.at[o], a_send.at[0], a_recv.at[o], partner).wait_recv()
-        total = total + jnp.dot(att_in[o], wo_all[o], preferred_element_type=f32)
+        total = total + jnp.dot(att_in[o], wo_all[o].reshape(width, model), preferred_element_type=f32)
     spread = jnp.mean(total * total, axis=-1, keepdims=True)
     out_ref[...] = (total * lax.rsqrt(spread + epsilon) * ogain_ref[...]).astype(bf)
 
-    for slot in (0, 1, 2, 4, 6):
-        x_full(tp, slot, partner).wait_send()
-    for slot in (3, 5, 7, 8):
-        x_half(tp, 0, slot, 0, partner).wait_send()
+    x_gather.drain()
+    w_gather.drain()
     for sent in mate_copies():
         sent.wait_send()
     for slab in range(2):
@@ -375,11 +437,10 @@
         def _():
             q_copy(d).wait_send()
     for d in range(1, chunks):
-        w_copy(tp, d).wait_send()
         a_copy(d).wait_send()
 
     def drained(source, t):
-        @pl.when((source >= z) & (source != z))
+        @pl.when((source > z) & jnp.logical_not(joined(source)))
         def _():
             for sent in out_copy(head, source):
                 sent.wait_send()
@@ -429,12 +490,12 @@
             pltpu.VMEM((ZN, 2, 1, block), f32),
             pltpu.VMEM((chunks, rows, width), bf),
             pltpu.VMEM((chunks, rows, width), bf),
-            pltpu.VMEM((chunks, width, model), bf),
-            dma((9,)), dma((chunks,)), dma((2, 2)), dma((2,)),
+            pltpu.VMEM((chunks, 2, width // 2, model), bf),
+            dma((14,)), dma((chunks, 2)), dma((2,)),
             dma((2, 3)), dma((2, XN)), dma((2, 3)), dma((2, XN)),
             dma((7,)), dma((ZN,)),
             dma((2, ZN)), dma((ZN, 2)), dma((2, ZN)), dma((ZN, 2)),
-            dma((7,)), dma((chunks,)), dma((7,)), dma((chunks,)),
+            dma((7,)), dma((chunks,)), dma((14,)), dma((chunks, 2)),
         ],
         compiler_params=pltpu.CompilerParams(collective_id=0, has_side_effects=True, vmem_limit_bytes=56 * 1024 * 1024),
     )(stop_offset, activations, input_gain[None], query_weight, key_weight, value_weight, output_weight, output_gain[None])

time: 65.5 us -> 64.3 us (0.982)
  Pallas kernels: 63.8 us -> 62.5 us
    pallas_call x1, Pallas kernels: 63.8 us -> 62.5 us  [local(): pl.pallas_call(layer_kernel, out_shape=jax.ShapeDtypeStruct((rows, model)...]
where the time goes in v4:
time: 64.3 us; the launch traced here: 64.1 us
  Pallas kernels  62.5 us (97%)
  local copies, waits for them, and re-layouts  1.57 us (2%)
    pallas_call x1, Pallas kernels, local(): pl.pallas_call(layer_kernel, out_shape=jax.ShapeDtypeStruct((rows, model)...  62.5 us
    unnamed x1, local copies, waits for them, and re-layouts  1.57 us

profile of v4, /device:TPU:231, one launch (start us, length us, event | category | flops | bytes accessed | tf_op | source)
XLA Modules:
  0.0 64.1 jit_solution(754277185235203513)
XLA Ops:
  0.0 62.5 %shard_map.82 = bf16[64,1024]{1,0:T(8,128)(2,1)} custom-call(f32[2]{0:T(128)} %off_ref.1, bf16[64,1024]{1,0:T(8,128)(2,1)} %x_ref.1, f32[1,1024]{1,0:T(1,128)} %bitcast.2, bf16[1024,128]{1,0:T(8,128)(2,1)} %wq_ref.1, bf16[1024,128]{1,0:T(8,128)(2,1)} %wk_ref.1, bf16[1024,128]{1,0:T(8,128)(2,1)} %wv_ref.1, bf16[128,1024]{1,0:T(8,128)(2,1)} %wo_ref.1, ...), custom_call_target="tpu_custom_call" | custom-call | tf_op jit(solution)/shard_map/pallas_call | solution.py:466
  62.5 1.6 %copy.10 = bf16[64,1024]{1,0:T(8,128)(2,1)} copy(bf16[64,1024]{1,0:T(8,128)(2,1)} %shard_map.82) | data formatting | bytes 262144

commit v5 on v4

--- a/solution.py
+++ b/solution.py
@@ -12,6 +12,15 @@
 XN, ZN, YN = 4, 8, 4
 LAST = ZN - 1
 Q_ORDER = (7, 6, 1, 5, 2, 4, 3)
+OWN_ORDER = (1, 7, 2, 6, 3, 5, 4)
+MATE_ORDER = (6, 2, 5, 3, 4, 7, 1, 0)
+
+
+def pick(values, index):
+    out = jnp.int32(values[0])
+    for position, value in enumerate(values[1:], 1):
+        out = jnp.where(index == position, jnp.int32(value), out)
+    return out
 
 
 def suffix_products(total):
@@ -44,8 +53,8 @@
 
 
 def layer_kernel(
-    off_ref, x_ref, gain_ref, wq_ref, wk_ref, wv_ref, wo_ref, ogain_ref, out_ref,
-    xall, wt, pk, pv_, qmine, kmate, vmate, qbuf, kt, vt, kop, qop, wa, wb, wc, wd, acc, carry,
+    off_ref, x_hbm, gain_hbm, wq_hbm, wk_hbm, wv_hbm, wo_hbm, ogain_hbm, out_ref,
+    x_ref, gain_ref, wq_ref, wk_ref, wv_ref, ogain_ref, in_sem, xall, wt, pk, pv_, qmine, kmate, vmate, qbuf, kt, vt, kop, qop, wa, wb, wc, wd, acc, carry,
     send_out, send_keep, ret_out, ret_keep, att, att_in, wo_all,
     x_send, x_recv, m_send, k_send, k_recv, v_send, v_recv, q_send, q_recv,
     ro_send, ro_recv, rk_send, rk_recv, a_send, a_recv, w_send, w_recv,
@@ -57,10 +66,10 @@
     head = lax.div(z, ZN // 2)
     other = 1 - head
     partner = (sp, y * 2 + 1 - c)
-    rows, model = x_ref.shape
+    rows, model = x_hbm.shape
     chunks = YN * 2
     block = rows * chunks
-    width = wq_ref.shape[1]
+    width = wq_hbm.shape[1]
     half = width // 2
     steps = block // SUB
     bf, f32 = jnp.bfloat16, jnp.float32
@@ -89,6 +98,19 @@
     peers += [at_z(lax.rem(z + d, ZN)) for d in range(1, ZN)]
     for peer in peers:
         pl.semaphore_signal(barrier, inc=1, device_id=peer, device_id_type=MESH)
+    weights_in = [
+        pltpu.make_async_copy(src, dst, in_sem.at[n])
+        for n, (src, dst) in enumerate(
+            (
+                (x_hbm, x_ref), (gain_hbm, gain_ref), (wq_hbm, wq_ref), (wk_hbm, wk_ref), (wv_hbm, wv_ref),
+                (wo_hbm.at[0 : width // 2], wo_all.at[tp, 0]), (wo_hbm.at[width // 2 :], wo_all.at[tp, 1]), (ogain_hbm, ogain_ref),
+            )
+        )
+    ]
+    for piece in weights_in:
+        piece.start()
+    weights_in[0].wait()
+    weights_in[1].wait()
     wide = x_ref[...].astype(f32)
     spread = jnp.mean(wide * wide, axis=-1, keepdims=True)
     xall[tp] = (wide * lax.rsqrt(spread + epsilon) * gain_ref[...]).astype(bf).reshape(xall.shape[1:])
@@ -143,7 +165,8 @@
     x_gather = TpGather(xall, x_send, x_recv)
     w_gather = TpGather(wo_all, w_send, w_recv)
     x_gather.begin()
-    wo_all[tp] = wo_ref[...].reshape(wo_all.shape[1:])
+    for piece in weights_in[2:]:
+        piece.wait()
 
     row = lax.broadcasted_iota(jnp.int32, (block, block), 0)
     col = lax.broadcasted_iota(jnp.int32, (1, block), 1)
@@ -331,7 +354,6 @@
     qbuf[z] = qmine[head]
     qop[0:half] = qmine[head]
     key_rows(head, x)
-    diagonal_tile(head)
     pass_on(head)
     k_copy(other, x, 0, partner).wait_recv()
     spread_keys(other)
@@ -339,35 +361,34 @@
     spread_values(other)
     beside(head)
     opposite(head)
-    w_gather.relay()
+    diagonal_tile(head)
     for d in range(1, XN):
         key_rows(head, along_x(d))
+    w_gather.relay()
     below_diagonal(head, z)
 
-    own_jobs = LAST - z
-
     def job(n, t):
-        @pl.when(n == jnp.minimum(2, own_jobs))
+        @pl.when(n == 2)
         def _():
             pass_on(other)
 
-        @pl.when(n == 3)
+        @pl.when(n == 5)
         def _():
             w_gather.relay_far()
 
-        @pl.when(n == own_jobs)
+        @pl.when(n == LAST)
         def _():
             beside(other)
             opposite(other)
             for d in range(XN):
                 key_rows(other, along_x(d))
 
-        @pl.when(n < LAST)
-        def _():
-            mine = n < own_jobs
-            slab = jnp.where(mine, head, other)
-            source = jnp.where(mine, z + 1 + n, n + 1)
-
+        mine = n < LAST
+        slab = jnp.where(mine, head, other)
+        source = jnp.where(mine, z + pick(OWN_ORDER, n), lax.rem(z + pick(MATE_ORDER, n - LAST), ZN))
+
+        @pl.when((source < ZN) & (mine | (source > mate)))
+        def _():
             @pl.when(mine | (source < z))
             def _():
                 q_arrived(source)
@@ -376,7 +397,7 @@
 
         return t
 
-    lax.fori_loop(0, ZN, job, 0)
+    lax.fori_loop(0, LAST + ZN, job, 0)
 
     @pl.when(upper)
     def _():
@@ -409,18 +430,25 @@
     lax.fori_loop(0, z + 1, gather, 0)
     att[...] = jnp.transpose(acc[...]).astype(bf).reshape(att.shape)
 
+    def lanes(core):
+        return pl.ds(pl.multiple_of(core * width, width), width)
+
     def a_copy(d):
         o = lax.rem(tp + d, chunks)
-        return copy(att.at[o], att_in.at[tp], a_send.at[d - 1], a_recv.at[tp], at_tp(o))
+        return copy(att.at[o], att_in.at[y, :, lanes(c)], a_send.at[d - 1], a_recv.at[tp], at_tp(o))
 
     for d in range(1, chunks):
         a_copy(d).start()
-    total = jnp.dot(att[tp], wo_ref[...], preferred_element_type=f32)
+    att_in[y, :, lanes(c)] = att[tp]
     w_gather.complete()
-    for d in range(1, chunks):
-        o = lax.rem(tp + d, chunks)
-        copy(att_in.at[o], att_in.at[o], a_send.at[0], a_recv.at[o], partner).wait_recv()
-        total = total + jnp.dot(att_in[o], wo_all[o].reshape(width, model), preferred_element_type=f32)
+    total = jnp.zeros((rows, model), f32)
+    for d in (0, 1, 3, 2):
+        pair = along_y(d)
+        for o in (pair * 2 + 1 - c,) if d == 0 else (pair * 2 + c, pair * 2 + 1 - c):
+            slot = att_in.at[pair, :, lanes(lax.rem(o, 2))]
+            copy(slot, slot, a_send.at[0], a_recv.at[o], partner).wait_recv()
+        both = wo_all[pl.ds(pair * 2, 2)].reshape(2 * width, model)
+        total = total + jnp.dot(att_in[pair], both, preferred_element_type=f32)
     spread = jnp.mean(total * total, axis=-1, keepdims=True)
     out_ref[...] = (total * lax.rsqrt(spread + epsilon) * ogain_ref[...]).astype(bf)
 
@@ -466,9 +494,14 @@
     return pl.pallas_call(
         layer_kernel,
         out_shape=jax.ShapeDtypeStruct((rows, model), bf),
-        in_specs=[pl.BlockSpec(memory_space=pltpu.SMEM)] + [vmem] * 7,
+        in_specs=[pl.BlockSpec(memory_space=pltpu.SMEM)] + [pl.BlockSpec(memory_space=pl.ANY)] * 7,
         out_specs=vmem,
         scratch_shapes=[
+            pltpu.VMEM((rows, model), bf),
+            pltpu.VMEM((1, model), f32),
+            *[pltpu.VMEM((model, width), bf)] * 3,
+            pltpu.VMEM((1, model), f32),
+            dma((8,)),
             pltpu.VMEM((chunks, 2, rows // 2, model), bf),
             pltpu.VMEM((3, width, model), bf),
             pltpu.VMEM((block, block), bf),
@@ -489,7 +522,7 @@
             pltpu.VMEM((ZN, 2, half, block), bf),
             pltpu.VMEM((ZN, 2, 1, block), f32),
             pltpu.VMEM((chunks, rows, width), bf),
-            pltpu.VMEM((chunks, rows, width), bf),
+            pltpu.VMEM((YN, rows, 2 * width), bf),
             pltpu.VMEM((chunks, 2, width // 2, model), bf),
             dma((14,)), dma((chunks, 2)), dma((2,)),
             dma((2, 3)), dma((2, XN)), dma((2, 3)), dma((2, XN)),

time: 64.3 us -> 62.2 us (0.967)
  Pallas kernels: 62.5 us -> 60.1 us
    pallas_call x1, Pallas kernels: 62.5 us -> 60.1 us  [local(): pl.pallas_call(layer_kernel, out_shape=jax.ShapeDtypeStruct((rows, model)...]
where the time goes in v5:
time: 62.2 us; the launch traced here: 61.7 us
  Pallas kernels  60.1 us (97%)
  local copies, waits for them, and re-layouts  1.57 us (3%)
    pallas_call x1, Pallas kernels, local(): pl.pallas_call(layer_kernel, out_shape=jax.ShapeDtypeStruct((rows, model)...  60.1 us
    unnamed x1, local copies, waits for them, and re-layouts  1.57 us

profile of v5, /device:TPU:231, one launch (start us, length us, event | category | flops | bytes accessed | tf_op | source)
XLA Modules:
  0.0 61.7 jit_solution(8201837381786925488)
XLA Ops:
  0.0 60.1 %shard_map.82 = bf16[64,1024]{1,0:T(8,128)(2,1)} custom-call(f32[2]{0:T(128)} %off_ref.1, bf16[64,1024]{1,0:T(8,128)(2,1)} %x_hbm.1, f32[1,1024]{1,0:T(1,128)} %bitcast.2, bf16[1024,128]{1,0:T(8,128)(2,1)} %wq_hbm.1, bf16[1024,128]{1,0:T(8,128)(2,1)} %wk_hbm.1, bf16[1024,128]{1,0:T(8,128)(2,1)} %wv_hbm.1, bf16[128,1024]{1,0:T(8,128)(2,1)} %wo_hbm.1, ...), custom_call_target="tpu_custom_call" | custom-call | tf_op jit(solution)/shard_map/pallas_call | solution.py:494
  60.1 1.6 %copy.10 = bf16[64,1024]{1,0:T(8,128)(2,1)} copy(bf16[64,1024]{1,0:T(8,128)(2,1)} %shard_map.82) | data formatting | bytes 262144

commit v6 on v5

--- a/solution.py
+++ b/solution.py
@@ -12,7 +12,7 @@
 XN, ZN, YN = 4, 8, 4
 LAST = ZN - 1
 Q_ORDER = (7, 6, 1, 5, 2, 4, 3)
-OWN_ORDER = (1, 7, 2, 6, 3, 5, 4)
+OWN_ORDER = (1, 7, 2, 6, 5, 4, 3)
 MATE_ORDER = (6, 2, 5, 3, 4, 7, 1, 0)
 
 
@@ -285,8 +285,8 @@
     def out_copy(slab, source):
         index = slab_index(slab, source)
         return (
+            copy(send_keep.at[slab, source], ret_keep.at[index, head], rk_send.at[slab, source], rk_recv.at[index, head], at_z(source)),
             copy(send_out.at[slab, source], ret_out.at[index, head], ro_send.at[slab, source], ro_recv.at[index, head], at_z(source)),
-            copy(send_keep.at[slab, source], ret_keep.at[index, head], rk_send.at[slab, source], rk_recv.at[index, head], at_z(source)),
         )
 
     def deliver(slab, source, part, keep):
@@ -368,7 +368,7 @@
     below_diagonal(head, z)
 
     def job(n, t):
-        @pl.when(n == 2)
+        @pl.when(n == jnp.where(z < 4, 3, 0))
         def _():
             pass_on(other)
 

time: 62.2 us -> 61.9 us (level)
  the two profiles are of different devices: /device:TPU:231 before, /device:TPU:129 now
where the time goes in v6:
time: 61.9 us; the launch traced here: 61.8 us
  Pallas kernels  60.2 us (97%)
  local copies, waits for them, and re-layouts  1.57 us (3%)
    pallas_call x1, Pallas kernels, local(): pl.pallas_call(layer_kernel, out_shape=jax.ShapeDtypeStruct((rows, model)...  60.2 us
    unnamed x1, local copies, waits for them, and re-layouts  1.57 us

profile of v6, /device:TPU:129, one launch (start us, length us, event | category | flops | bytes accessed | tf_op | source)
XLA Modules:
  0.0 61.8 jit_solution(1493661976036035786)
XLA Ops:
  0.0 60.2 %shard_map.82 = bf16[64,1024]{1,0:T(8,128)(2,1)} custom-call(f32[2]{0:T(128)} %off_ref.1, bf16[64,1024]{1,0:T(8,128)(2,1)} %x_hbm.1, f32[1,1024]{1,0:T(1,128)} %bitcast.2, bf16[1024,128]{1,0:T(8,128)(2,1)} %wq_hbm.1, bf16[1024,128]{1,0:T(8,128)(2,1)} %wk_hbm.1, bf16[1024,128]{1,0:T(8,128)(2,1)} %wv_hbm.1, bf16[128,1024]{1,0:T(8,128)(2,1)} %wo_hbm.1, ...), custom_call_target="tpu_custom_call" | custom-call | tf_op jit(solution)/shard_map/pallas_call | solution.py:494
  60.2 1.6 %copy.10 = bf16[64,1024]{1,0:T(8,128)(2,1)} copy(bf16[64,1024]{1,0:T(8,128)(2,1)} %shard_map.82) | data formatting | bytes 262144
